TPU v7x, 128 devices: a whole 4x4x4 slice. The times are simulated.
128 devices in a mesh: sp: 16 (over z, x), fs: 4 (over y), tp: 2 (over core).
Axes of the slice: x: 4, y: 4, z: 4, core: 2. Of those that a mesh axis runs over, the one named last changes fastest.
Arguments:
- stream: bfloat16 [4, 16384, 2048], P('fs', 'sp', 'tp'), parts along dimension 0, may hold values from -6 to 6
- w_pool_in: bfloat16 [2048, 1024], P(None, 'tp'), may hold values from -0.125 to 0.125
- w_query: bfloat16 [2048, 1024], P(None, 'tp'), may hold values from -0.125 to 0.125
- w_forget: bfloat16 [2048, 1024], P(None, 'tp'), may hold values from -0.125 to 0.125
- w_value: bfloat16 [2048, 1024], P(None, 'tp'), may hold values from -0.125 to 0.125
- w_outgate: bfloat16 [2048, 1024], P(None, 'tp'), may hold values from -0.125 to 0.125
- pool_mix: bfloat16 [4, 256, 256], P('tp'), may hold values from -0.375 to 0.375
- pool_scale: float32 [1024], P('tp'), may hold values from 0.1 to 1.9
- lower_bound: float32 [1024], P('tp'), may hold values from 0.9 to 1
- extra_decay: float32 [16384, 8], P('sp', 'tp'), may hold values from -0.7 to 0
- rec_gain: float32 [128], replicated, may hold values from 0.1 to 1.9
- w_out_pool: bfloat16 [1024, 2048], P('tp'), may hold values from -0.125 to 0.125
- w_out_rec: bfloat16 [1024, 2048], P('tp'), may hold values from -0.125 to 0.125
- norm_gain: float32 [2048], P('tp'), may hold values from 0.1 to 1.9
- norm_bias: float32 [2048], P('tp'), may hold values from -3 to 3
Outputs:
- layer_out: bfloat16 [4, 16384, 2048], P('fs', 'sp', 'tp'), parts along dimension 0
There are 4 independent parts, one for each index of `fs`. A program takes and returns all parts, laid end to end along the dimension named above; an argument that names none is the same for every part. Nothing has to cross between parts.
All inputs are finite; a program needn't handle non-finite values.
Results may differ from a plain program's by a relative error of at most 0.0085.
Values may be sent and summed in bfloat16 or wider, within the bound.
A program may use at most 128 MiB of HBM per device.

v0:
```python
import functools

import jax
import jax.numpy as jnp
from jax import lax
from jax.experimental import pallas as pl
from jax.experimental.pallas import tpu as pltpu
from jax.sharding import PartitionSpec as P

DK = 128
BLOCK_ROWS = 128
GROUP_CH = 256
HALO = 16
LANES = 128

ALPHA = 2.0**0.25
EPS_RMS = 1e-06
EPS_NORM = 1e-05
F32 = jnp.float32
BF16 = jnp.bfloat16
NT = (((1,), (1,)), ((), ()))
TN = (((0,), (0,)), ((), ()))


def dot(a, b, dims=None):
    if dims is None:
        return jnp.dot(a, b, preferred_element_type=F32)
    return lax.dot_general(a, b, dims, preferred_element_type=F32)


def half_sigmoid(x):
    return 0.5 + 0.5 * jnp.tanh(0.5 * x)


def mixer(
    n_sp, n_tp, rows_x,
    stream, w_pool, w_query, w_forget, w_value, w_gate,
    mix_in, scale_in, bound_in, extra_in, gain_in, wo_pool, wo_rec,
    out, stats,
    x_buf, w_buf, wo_buf, a_buf, v_buf, u_buf, e_buf, t_buf, p_buf, q_buf, g_buf, r_buf,
    o_buf, half_buf, state, state_out, state_in, halo_in, stat_own, stat_peer, stat_sum,
    mix, scale, bound, extra, gain,
    x_loc, x_send, x_recv, w_sem, wo_loc, wo_send, wo_recv, a_send, a_recv,
    st_send, st_recv, h_send, h_recv, s_send, s_recv, o_sem, t_sem, small_sem,
):
    sp, tp = lax.axis_index("sp"), lax.axis_index("tp")
    peer = 1 - tp
    length, feats = stream.shape[1], stream.shape[2]
    chans = bound.shape[1]
    heads = chans // DK
    pool_w = scale.shape[1]
    groups = mix.shape[0]
    chunks = length // rows_x
    blocks = length // BLOCK_ROWS
    per = rows_x // BLOCK_ROWS

    def x_in(c):
        rows = pl.ds(c * rows_x, rows_x)
        return pltpu.make_async_copy(stream.at[0, rows], x_buf.at[tp, rows], x_loc.at[c])

    def x_out(c):
        rows = pl.ds(c * rows_x, rows_x)
        return pltpu.make_async_remote_copy(
            x_buf.at[tp, rows], x_buf.at[tp, rows], x_send.at[c], x_recv.at[c],
            device_id={"tp": peer}, device_id_type=pl.DeviceIdType.MESH)

    def w_in(i):
        src = (w_forget, w_value, w_pool, w_query, w_gate)[i]
        return [
            pltpu.make_async_copy(src.at[pl.ds(k * feats, feats)], w_buf.at[i, k], w_sem.at[i, k])
            for k in range(n_tp)
        ]

    my_cols = pl.ds(pl.multiple_of(tp * feats, LANES), feats)
    peer_cols = pl.ds(pl.multiple_of(peer * feats, LANES), feats)
    wo_places = ((wo_pool, pl.ds(0, pool_w)), (wo_rec, pl.ds(pool_w, chans)))

    def wo_in(i):
        src, place = wo_places[i]
        return pltpu.make_async_copy(src.at[:, my_cols], wo_buf.at[tp, place], wo_loc.at[i])

    def wo_out(i):
        src, place = wo_places[i]
        return pltpu.make_async_remote_copy(
            src.at[:, peer_cols], wo_buf.at[tp, place], wo_send.at[i], wo_recv.at[i],
            device_id={"tp": peer}, device_id_type=pl.DeviceIdType.MESH)

    def a_out(i, c):
        rows, cols = pl.ds(c * rows_x, rows_x), wo_places[i][1]
        return pltpu.make_async_remote_copy(
            a_buf.at[tp, rows, cols], a_buf.at[tp, rows, cols], a_send.at[i, c], a_recv.at[i, c],
            device_id={"tp": peer}, device_id_type=pl.DeviceIdType.MESH)

    def st_out(k, slot):
        return pltpu.make_async_remote_copy(
            state_out, state_in.at[slot], st_send.at[k], st_recv.at[slot],
            device_id={"sp": k}, device_id_type=pl.DeviceIdType.MESH)

    def h_out(k):
        return pltpu.make_async_remote_copy(
            p_buf.at[pl.ds(BLOCK_ROWS + length - HALO, HALO)], halo_in, h_send, h_recv,
            device_id={"sp": k}, device_id_type=pl.DeviceIdType.MESH)

    def s_out(c):
        return pltpu.make_async_remote_copy(
            stat_own.at[c], stat_peer.at[c], s_send.at[c], s_recv.at[c],
            device_id={"tp": peer}, device_id_type=pl.DeviceIdType.MESH)

    def o_out(c):
        rows = pl.ds(c * rows_x, rows_x)
        return pltpu.make_async_copy(o_buf.at[rows], out.at[rows], o_sem.at[c])

    def t_out(c):
        rows = pl.ds(c * rows_x, rows_x)
        return pltpu.make_async_copy(stat_sum.at[c], stats.at[rows], t_sem.at[c])

    smalls = [
        pltpu.make_async_copy(src, dst, small_sem.at[i])
        for i, (src, dst) in enumerate(
            ((bound_in, bound), (extra_in, extra), (mix_in, mix), (scale_in, scale), (gain_in, gain)))
    ]

    for c in range(chunks):
        x_in(c).start()
        if c == 0:
            for i in (0, 1):
                for copy in w_in(i):
                    copy.start()
            for copy in smalls:
                copy.start()

    barrier = pltpu.get_barrier_semaphore()
    pl.semaphore_signal(barrier, inc=1, device_id={"tp": peer}, device_id_type=pl.DeviceIdType.MESH)
    for step in range(1, n_sp):
        pl.semaphore_signal(
            barrier, inc=1, device_id={"sp": lax.rem(sp + step, n_sp)},
            device_id_type=pl.DeviceIdType.MESH)
    p_buf[pl.ds(0, BLOCK_ROWS), :] = jnp.zeros((BLOCK_ROWS, pool_w), BF16)
    state[...] = jnp.zeros_like(state)
    pl.semaphore_wait(barrier, n_sp)

    for c in range(chunks):
        x_in(c).wait()
        x_out(c).start()

    row_ids = lax.broadcasted_iota(jnp.int32, (BLOCK_ROWS, BLOCK_ROWS), 0)
    col_ids = lax.broadcasted_iota(jnp.int32, (BLOCK_ROWS, BLOCK_ROWS), 1)
    lower = row_ids >= col_ids
    tri = jnp.where(lower, 1.0, 0.0).astype(BF16)
    lower_twice = jnp.concatenate([row_ids, row_ids], axis=1) >= jnp.concatenate([col_ids, col_ids], axis=1)
    tri_twice = jnp.concatenate([tri, tri], axis=1)
    ones = jnp.ones((2 * BLOCK_ROWS, DK), BF16)

    for i in (0, 1):
        for copy in w_in(i):
            copy.wait()
    for copy in smalls:
        copy.wait()
    for i in (2, 3, 4):
        for copy in w_in(i):
            copy.start()
    for i in range(2):
        wo_in(i).start()
        wo_out(i).start()

    def first(c, _):
        rows = pl.ds(pl.multiple_of(c * rows_x, rows_x), rows_x)
        own = x_buf[tp, rows]
        f_own = dot(own, w_buf[0, tp])
        v_own = dot(own, w_buf[1, tp])
        x_out(c).wait_recv()
        other = x_buf[peer, rows]
        f_in = (f_own + dot(other, w_buf[0, peer])).astype(BF16).astype(F32)
        vals = (v_own + dot(other, w_buf[1, peer])).astype(BF16)
        v_buf[rows, :] = vals
        open_part = 1.0 - bound[...]
        for j in range(per):
            part = slice(j * BLOCK_ROWS, (j + 1) * BLOCK_ROWS)
            b = c * per + j
            brows = pl.ds(pl.multiple_of(b * BLOCK_ROWS, BLOCK_ROWS), BLOCK_ROWS)
            weight = open_part * (0.5 - 0.5 * jnp.tanh(0.5 * f_in[part]))
            keep = jnp.log(1.0 - weight)
            high = keep.astype(BF16)
            low = (keep - high.astype(F32)).astype(BF16)
            drop = extra[:, brows]
            drop_high = drop.astype(BF16).astype(F32)
            drop_low = drop - drop_high
            drops = []
            for h in range(heads):
                pair = jnp.concatenate([drop_high[h:h + 1], drop_low[h:h + 1]], axis=1)
                wide = jnp.where(lower_twice, jnp.broadcast_to(pair, (BLOCK_ROWS, 2 * BLOCK_ROWS)), 0.0)
                drops.append(dot(wide.astype(BF16), ones))
            total = dot(tri_twice, jnp.concatenate([high, low], axis=0)) + jnp.concatenate(drops, axis=1)
            middle = 0.5 * total[BLOCK_ROWS - 1:BLOCK_ROWS]
            e_buf[brows, :] = jnp.exp(total - middle)
            down = (weight * jnp.exp(middle - total)).astype(BF16)
            u_buf[brows, :] = down
            half = jnp.exp(middle)
            half_buf[b] = jnp.broadcast_to(half, (8, chans))
            for h in range(heads):
                lanes = slice(h * DK, (h + 1) * DK)
                hh = half[:, lanes]
                term = dot(vals[part, lanes], down[:, lanes], TN) * hh
                t_buf[b, :, lanes] = term
                state[:, lanes] = hh * hh * state[:, lanes] + term
        return 0

    lax.fori_loop(0, chunks, first, 0)

    for copy in w_in(2):
        copy.wait()

    def second(c, _):
        start = c * rows_x if isinstance(c, int) else pl.multiple_of(c * rows_x, rows_x)
        rows = pl.ds(start, rows_x)
        pooled = dot(x_buf[tp, rows], w_buf[2, tp]) + dot(x_buf[peer, rows], w_buf[2, peer])
        p_buf[pl.ds(start + BLOCK_ROWS, rows_x), :] = pooled.astype(BF16)
        return 0

    second(chunks - 1, 0)

    @pl.when(sp + 1 < n_sp)
    def _():
        h_out(sp + 1).start()

    log_half = half_buf[0, 0:1]
    for b in range(1, blocks):
        log_half = log_half * half_buf[b, 0:1]
    state_out[pl.ds(0, DK), :] = state[...].astype(BF16)
    state_out[pl.ds(DK, HALO), :] = jnp.broadcast_to(log_half * log_half, (HALO, chans)).astype(BF16)

    def send_state(k, _):
        st_out(k, sp).start()
        return 0

    lax.fori_loop(sp + 1, n_sp, send_state, 0)

    lax.fori_loop(0, chunks - 1, second, 0)

    for i in (3, 4):
        for copy in w_in(i):
            copy.wait()

    wide_rows = lax.broadcasted_iota(jnp.int32, (BLOCK_ROWS, 2 * BLOCK_ROWS), 0) + BLOCK_ROWS
    wide_cols = lax.broadcasted_iota(jnp.int32, (BLOCK_ROWS, 2 * BLOCK_ROWS), 1)
    back = wide_rows - wide_cols
    count = lax.broadcasted_iota(jnp.int32, (BLOCK_ROWS, LANES), 0) + (sp * length + 1)

    def third(step, _):
        c = chunks - 1 - step

        @pl.when((step == chunks - 1) & (sp > 0))
        def _():
            h_out(sp).wait_recv()
            p_buf[pl.ds(BLOCK_ROWS - HALO, HALO), :] = halo_in[...]

        rows = pl.ds(pl.multiple_of(c * rows_x, rows_x), rows_x)
        own, other = x_buf[tp, rows], x_buf[peer, rows]
        q_in = (dot(own, w_buf[3, tp]) + dot(other, w_buf[3, peer])).astype(BF16).astype(F32)
        ups = (q_in * half_sigmoid(q_in) * e_buf[rows, :]).astype(BF16)
        q_buf[rows, :] = ups
        g_in = dot(own, w_buf[4, tp]) + dot(other, w_buf[4, peer])
        g_buf[rows, :] = g_in.astype(BF16)
        for k in range(per):
            start = pl.multiple_of(c * rows_x + k * BLOCK_ROWS, BLOCK_ROWS)
            brows = pl.ds(start, BLOCK_ROWS)
            near = p_buf[pl.ds(start, 2 * BLOCK_ROWS), :]
            for j in range(groups):
                lanes = slice(j * GROUP_CH, (j + 1) * GROUP_CH)
                window = jnp.left_shift(jnp.int32(2), tp * groups + j)
                band = jnp.where((back >= 0) & (back < window), 1.0, 0.0).astype(BF16)
                share = 1.0 / jnp.minimum(count + start, window).astype(F32)
                share = jnp.concatenate([share] * (GROUP_CH // LANES), axis=1)
                sums = dot(band, near[:, lanes])
                diff = (sums * share - near[BLOCK_ROWS:, lanes].astype(F32)).astype(BF16)
                a_buf[tp, brows, lanes] = (dot(diff, mix[j]) * scale[:, lanes]).astype(BF16)
            for h in range(heads):
                lanes = slice(h * DK, (h + 1) * DK)
                up = ups[k * BLOCK_ROWS:(k + 1) * BLOCK_ROWS, lanes]
                scores = jnp.where(lower, dot(up, u_buf[brows, lanes], NT), 0.0).astype(BF16)
                e_buf[brows, lanes] = dot(scores, v_buf[brows, lanes])
        a_out(0, c).start()
        return 0

    lax.fori_loop(0, chunks, third, 0)

    for i in range(2):
        wo_in(i).wait()
        wo_out(i).wait_recv()

    pool_at, rec_at = wo_places[0][1], wo_places[1][1]

    def pool_part(step, _):
        c = chunks - 1 - step
        rows = pl.ds(pl.multiple_of(c * rows_x, rows_x), rows_x)
        mine = dot(a_buf[tp, rows, pool_at], wo_buf[tp, pool_at]) + ALPHA * x_buf[tp, rows].astype(F32)
        a_out(0, c).wait_recv()
        r_buf[rows, :] = mine + dot(a_buf[peer, rows, pool_at], wo_buf[peer, pool_at])
        return 0

    lax.fori_loop(0, chunks, pool_part, 0)

    state[...] = jnp.zeros_like(state)

    def join(k, _):
        st_out(sp, k).wait_recv()
        keep = state_in[k, pl.ds(DK, HALO), :].astype(F32)[0:1]
        state[...] = keep * state[...] + state_in[k, pl.ds(0, DK), :].astype(F32)
        return 0

    lax.fori_loop(0, sp, join, 0)

    def fourth(c, _):
        for k in range(per):
            b = c * per + k
            rows = pl.ds(pl.multiple_of(b * BLOCK_ROWS, BLOCK_ROWS), BLOCK_ROWS)
            half = half_buf[b, 0:1]
            before = state[...] * half
            carried = before.astype(BF16)
            state[...] = before * half + t_buf[b]
            for h in range(heads):
                lanes = slice(h * DK, (h + 1) * DK)
                raw = e_buf[rows, lanes] + dot(q_buf[rows, lanes], carried[:, lanes], NT)
                power = jnp.mean(raw * raw, axis=-1, keepdims=True)
                gate = g_buf[rows, lanes].astype(F32)
                rec = raw * lax.rsqrt(power + EPS_RMS) * gain[...] * (gate * half_sigmoid(gate))
                a_buf[tp, rows, pool_w + h * DK:pool_w + (h + 1) * DK] = rec.astype(BF16)
        a_out(1, c).start()
        return 0

    lax.fori_loop(0, chunks, fourth, 0)

    def fold(x):
        acc = x[:, :LANES]
        for k in range(1, feats // LANES):
            acc = acc + x[:, k * LANES:(k + 1) * LANES]
        return acc

    first_half = lax.broadcasted_iota(jnp.int32, (rows_x, LANES), 1) < LANES // 2

    def fifth(c, _):
        rows = pl.ds(pl.multiple_of(c * rows_x, rows_x), rows_x)
        mine = r_buf[rows, :] + dot(a_buf[tp, rows, rec_at], wo_buf[tp, rec_at])
        a_out(1, c).wait_recv()
        resid = mine + dot(a_buf[peer, rows, rec_at], wo_buf[peer, rec_at])
        o_buf[rows, :] = resid.astype(BF16)
        sums, squares = fold(resid), fold(resid * resid)
        sums = sums + pltpu.roll(sums, LANES // 2, 1)
        squares = squares + pltpu.roll(squares, LANES // 2, 1)
        stat_own[c] = jnp.where(first_half, sums, squares)
        s_out(c).start()
        o_out(c).start()
        return 0

    lax.fori_loop(0, chunks, fifth, 0)

    for c in range(chunks):
        s_out(c).wait_recv()
        stat_sum[c] = stat_own[c] + stat_peer[c]
        t_out(c).start()

    for c in range(chunks):
        x_out(c).wait_send()
        s_out(c).wait_send()
        o_out(c).wait()
        t_out(c).wait()
        for i in range(2):
            a_out(i, c).wait_send()
    for i in range(2):
        wo_out(i).wait_send()

    def sent_state(k, _):
        st_out(k, sp).wait_send()
        return 0

    lax.fori_loop(sp + 1, n_sp, sent_state, 0)

    @pl.when(sp + 1 < n_sp)
    def _():
        h_out(sp + 1).wait_send()


def finish(width, rows, resid, stats, norm_gain, norm_bias, out,
           r_buf, s_buf, o_buf, gain, bias, r_sem, s_sem, o_sem, n_sem):
    pieces = resid.shape[0] // rows

    def copies(c):
        part = pl.ds(c * rows, rows)
        return (
            pltpu.make_async_copy(stats.at[part], s_buf.at[part], s_sem.at[c]),
            pltpu.make_async_copy(resid.at[part], r_buf.at[part], r_sem.at[c]),
            pltpu.make_async_copy(o_buf.at[part], out.at[0, part], o_sem.at[c]),
        )

    norms = (
        pltpu.make_async_copy(norm_gain, gain, n_sem.at[0]),
        pltpu.make_async_copy(norm_bias, bias, n_sem.at[1]),
    )
    for copy in norms:
        copy.start()
    for c in range(pieces):
        for copy in copies(c)[:2]:
            copy.start()
    for copy in norms:
        copy.wait()
    first_half = lax.broadcasted_iota(jnp.int32, (rows, LANES), 1) < LANES // 2
    for c in range(pieces):
        part = pl.ds(c * rows, rows)
        for copy in copies(c)[:2]:
            copy.wait()
        both = s_buf[part, :]
        mean = jnp.sum(jnp.where(first_half, both, 0.0), axis=1, keepdims=True) / width
        square = jnp.sum(jnp.where(first_half, 0.0, both), axis=1, keepdims=True) / width
        inv = lax.rsqrt(square - mean * mean + EPS_NORM)
        o_buf[part, :] = ((r_buf[part, :].astype(F32) - mean) * inv * gain[...] + bias[...]).astype(BF16)
        copies(c)[2].start()
    for c in range(pieces):
        copies(c)[2].wait()


def solution(mesh):
    n_sp, n_tp = mesh.shape["sp"], mesh.shape["tp"]

    def local(stream, w_pool, w_query, w_forget, w_value, w_gate, mix, scale, bound, extra,
              gain, wo_pool, wo_rec, norm_gain, norm_bias):
        length, feats = stream.shape[1], stream.shape[2]
        chans, pool_w = bound.shape[0], scale.shape[0]
        blocks = length // BLOCK_ROWS
        rows_x = 256
        chunks = length // rows_x
        hbm = pl.BlockSpec(memory_space=pl.ANY)
        dma = pltpu.SemaphoreType.DMA
        scratch = [
            pltpu.VMEM((n_tp, length, feats), BF16),
            pltpu.VMEM((5, n_tp, feats, chans), BF16),
            pltpu.VMEM((n_tp, pool_w + chans, feats), BF16),
            pltpu.VMEM((n_tp, length, pool_w + chans), BF16),
            pltpu.VMEM((length, chans), BF16),
            pltpu.VMEM((length, chans), BF16),
            pltpu.VMEM((length, chans), F32),
            pltpu.VMEM((blocks, DK, chans), F32),
            pltpu.VMEM((BLOCK_ROWS + length, pool_w), BF16),
            pltpu.VMEM((length, chans), BF16),
            pltpu.VMEM((length, chans), BF16),
            pltpu.VMEM((length, feats), F32),
            pltpu.VMEM((length, feats), BF16),
            pltpu.VMEM((blocks, 8, chans), F32),
            pltpu.VMEM((DK, chans), F32),
            pltpu.VMEM((DK + HALO, chans), BF16),
            pltpu.VMEM((n_sp, DK + HALO, chans), BF16),
            pltpu.VMEM((HALO, pool_w), BF16),
            pltpu.VMEM((chunks, rows_x, LANES), F32),
            pltpu.VMEM((chunks, rows_x, LANES), F32),
            pltpu.VMEM((chunks, rows_x, LANES), F32),
            pltpu.VMEM(mix.shape, BF16),
            pltpu.VMEM((1, pool_w), F32),
            pltpu.VMEM((1, chans), F32),
            pltpu.VMEM((chans // DK, length), F32),
            pltpu.VMEM((1, DK), F32),
            dma((chunks,)), dma((chunks,)), dma((chunks,)), dma((5, n_tp)),
            dma((2,)), dma((2,)), dma((2,)), dma((2, chunks)), dma((2, chunks)),
            dma((n_sp,)), dma((n_sp,)), dma, dma, dma((chunks,)), dma((chunks,)), dma((chunks,)),
            dma((chunks,)), dma((5,)),
        ]
        row = lambda x: x.reshape(1, -1)
        resid, stats = pl.pallas_call(
            functools.partial(mixer, n_sp, n_tp, rows_x),
            out_shape=(
                jax.ShapeDtypeStruct((length, feats), BF16), jax.ShapeDtypeStruct((length, LANES), F32)),
            in_specs=[hbm] * 13,
            out_specs=(hbm, hbm),
            scratch_shapes=scratch,
            compiler_params=pltpu.CompilerParams(
                collective_id=0, has_side_effects=True, vmem_limit_bytes=60 * 1024 * 1024),
            name="mixer",
        )(stream, w_pool, w_query, w_forget, w_value, w_gate, mix, row(scale), row(bound), extra.T,
          row(gain), wo_pool, wo_rec)
        piece = 128
        pieces = length // piece
        return pl.pallas_call(
            functools.partial(finish, n_tp * feats, piece),
            out_shape=jax.ShapeDtypeStruct(stream.shape, BF16),
            in_specs=[hbm] * 4,
            out_specs=hbm,
            scratch_shapes=[
                pltpu.VMEM((length, feats), BF16),
                pltpu.VMEM((length, LANES), F32),
                pltpu.VMEM((length, feats), BF16),
                pltpu.VMEM((1, feats), F32),
                pltpu.VMEM((1, feats), F32),
                dma((pieces,)), dma((pieces,)), dma((pieces,)), dma((2,)),
            ],
            compiler_params=pltpu.CompilerParams(vmem_limit_bytes=60 * 1024 * 1024),
            name="finish",
        )(resid, stats, row(norm_gain), row(norm_bias))

    placed = (
        P("fs", "sp", "tp"), P(None, "tp"), P(None, "tp"), P(None, "tp"), P(None, "tp"),
        P(None, "tp"), P("tp", None, None), P("tp"), P("tp"), P("sp", "tp"), P(),
        P("tp", None), P("tp", None), P("tp"), P("tp"),
    )
    return jax.shard_map(
        local, mesh=mesh, in_specs=placed, out_specs=P("fs", "sp", "tp"), check_vma=False
    )
```

profile of v0, /device:TPU:119, one launch (start us, length us, event | category | flops | bytes accessed | tf_op | source)
XLA Modules:
  0.0 63.0 jit_solution(12967004553096799732)
XLA Ops:
  0.0 59.1 %mixer.1 = (bf16[1024,1024]{1,0:T(8,128)(2,1)}, f32[1024,128]{1,0:T(8,128)}) custom-call(bf16[1,1024,1024]{2,1,0:T(8,128)(2,1)} %stream.1, bf16[2048,512]{1,0:T(8,128)(2,1)} %w_pool.1, bf16[2048,512]{1,0:T(8,128)(2,1)} %w_query.1, bf16[2048,512]{1,0:T(8,128)(2,1)} %w_forget.1, bf16[2048,512]{1,0:T(8,128)(2,1)} %w_value.1, bf16[2048,512]{1,0:T(8,128)(2,1)} %w_gate.1, ...), custom_call_target="tpu_custom_call" | custom-call | tf_op jit(solution)/shard_map/mixer/pallas_call | solution.py:466
  59.1 3.8 %finish.1 = bf16[1,1024,1024]{2,1,0:T(8,128)(2,1)} custom-call(bf16[1024,1024]{1,0:T(8,128)(2,1)} %get-tuple-element.7.resid, f32[1024,128]{1,0:T(8,128)} %get-tuple-element.8.stats, f32[1,1024]{1,0:T(1,128)} %bitcast.7, f32[1,1024]{1,0:T(1,128)} %bitcast.8), custom_call_target="tpu_custom_call" | custom-call | tf_op jit(solution)/shard_map/finish/pallas_call | solution.py:480
where the time goes:
time: 63.1 us; the launch traced here: 63 us
  Pallas kernels  63 us (100%)
    pallas_call x1, Pallas kernels, local(): pl.pallas_call(functools.partial(mixer, n_sp, n_tp, rows_x), out_shape=(j...  59.1 us
    pallas_call x1, Pallas kernels, local(): pl.pallas_call(functools.partial(finish, n_tp * feats, piece), out_shape=...  3.84 us

commit v1 on v0

--- a/solution.py
+++ b/solution.py
@@ -38,10 +38,10 @@
     mix_in, scale_in, bound_in, extra_in, gain_in, wo_pool, wo_rec,
     out, stats,
     x_buf, w_buf, wo_buf, a_buf, v_buf, u_buf, e_buf, t_buf, p_buf, q_buf, g_buf, r_buf,
-    o_buf, half_buf, state, state_out, state_in, halo_in, stat_own, stat_peer, stat_sum,
+    o_buf, half_buf, state, mine_out, row_in, total_out, total_in, start_out, start_in, halo_in, stat_own, stat_peer, stat_sum,
     mix, scale, bound, extra, gain,
     x_loc, x_send, x_recv, w_sem, wo_loc, wo_send, wo_recv, a_send, a_recv,
-    st_send, st_recv, h_send, h_recv, s_send, s_recv, o_sem, t_sem, small_sem,
+    m_send, m_recv, r_send, r_recv, b_send, b_recv, h_send, h_recv, s_send, s_recv, o_sem, t_sem, small_sem,
 ):
     sp, tp = lax.axis_index("sp"), lax.axis_index("tp")
     peer = 1 - tp
@@ -53,6 +53,10 @@
     chunks = length // rows_x
     blocks = length // BLOCK_ROWS
     per = rows_x // BLOCK_ROWS
+    row_n = heads
+    col_n = n_sp // row_n
+    x_at, z_at = lax.rem(sp, row_n), lax.div(sp, row_n)
+    row0 = z_at * row_n
 
     def x_in(c):
         rows = pl.ds(c * rows_x, rows_x)
@@ -91,10 +95,31 @@
             a_buf.at[tp, rows, cols], a_buf.at[tp, rows, cols], a_send.at[i, c], a_recv.at[i, c],
             device_id={"tp": peer}, device_id_type=pl.DeviceIdType.MESH)
 
-    def st_out(k, slot):
-        return pltpu.make_async_remote_copy(
-            state_out, state_in.at[slot], st_send.at[k], st_recv.at[slot],
-            device_id={"sp": k}, device_id_type=pl.DeviceIdType.MESH)
+    def mine_to(k, slot):
+        return pltpu.make_async_remote_copy(
+            mine_out.at[k], row_in.at[slot], m_send.at[k], m_recv.at[slot],
+            device_id={"sp": row0 + k}, device_id_type=pl.DeviceIdType.MESH)
+
+    def total_to(k, slot):
+        return pltpu.make_async_remote_copy(
+            total_out, total_in.at[slot], r_send.at[k], r_recv.at[slot],
+            device_id={"sp": k * row_n + x_at}, device_id_type=pl.DeviceIdType.MESH)
+
+    def start_to(k, slot):
+        return pltpu.make_async_remote_copy(
+            start_out.at[k], start_in.at[slot], b_send.at[k], b_recv.at[slot],
+            device_id={"sp": row0 + k}, device_id_type=pl.DeviceIdType.MESH)
+
+    def greet(k):
+        pl.semaphore_signal(
+            barrier, inc=1, device_id={"sp": k}, device_id_type=pl.DeviceIdType.MESH)
+
+    def each(low, high, do):
+        def step(k, _):
+            do(k)
+            return 0
+
+        lax.fori_loop(low, high, step, 0)
 
     def h_out(k):
         return pltpu.make_async_remote_copy(
@@ -131,13 +156,17 @@
 
     barrier = pltpu.get_barrier_semaphore()
     pl.semaphore_signal(barrier, inc=1, device_id={"tp": peer}, device_id_type=pl.DeviceIdType.MESH)
-    for step in range(1, n_sp):
-        pl.semaphore_signal(
-            barrier, inc=1, device_id={"sp": lax.rem(sp + step, n_sp)},
-            device_id_type=pl.DeviceIdType.MESH)
     p_buf[pl.ds(0, BLOCK_ROWS), :] = jnp.zeros((BLOCK_ROWS, pool_w), BF16)
     state[...] = jnp.zeros_like(state)
-    pl.semaphore_wait(barrier, n_sp)
+    with jax.named_scope("entry"):
+        pl.semaphore_wait(barrier, 1 + x_at + z_at)
+    for step in range(1, row_n):
+        greet(row0 + lax.rem(x_at + step, row_n))
+    for step in range(1, col_n):
+        greet(lax.rem(z_at + step, col_n) * row_n + x_at)
+    leads = (x_at == 0) & (z_at > 0)
+    ends = (x_at == row_n - 1) & (z_at < col_n - 1)
+    later = (row_n - 1 - x_at) + (col_n - 1 - z_at) + jnp.where(ends, 1, 0)
 
     for c in range(chunks):
         x_in(c).wait()
@@ -164,6 +193,12 @@
         wo_out(i).start()
 
     def first(c, _):
+        @pl.when((c == 1) & leads)
+        def _():
+            with jax.named_scope("lead"):
+                pl.semaphore_wait(barrier, later)
+            greet(sp - 1)
+
         rows = pl.ds(pl.multiple_of(c * rows_x, rows_x), rows_x)
         own = x_buf[tp, rows]
         f_own = dot(own, w_buf[0, tp])
@@ -205,7 +240,8 @@
                 state[:, lanes] = hh * hh * state[:, lanes] + term
         return 0
 
-    lax.fori_loop(0, chunks, first, 0)
+    with jax.named_scope("L_first"):
+        lax.fori_loop(0, chunks, first, 0)
 
     for copy in w_in(2):
         copy.wait()
@@ -219,6 +255,11 @@
 
     second(chunks - 1, 0)
 
+    @pl.when(jnp.logical_not(leads) & (sp + 1 < n_sp))
+    def _():
+        with jax.named_scope("later"):
+            pl.semaphore_wait(barrier, later)
+
     @pl.when(sp + 1 < n_sp)
     def _():
         h_out(sp + 1).start()
@@ -226,16 +267,17 @@
     log_half = half_buf[0, 0:1]
     for b in range(1, blocks):
         log_half = log_half * half_buf[b, 0:1]
-    state_out[pl.ds(0, DK), :] = state[...].astype(BF16)
-    state_out[pl.ds(DK, HALO), :] = jnp.broadcast_to(log_half * log_half, (HALO, chans)).astype(BF16)
-
-    def send_state(k, _):
-        st_out(k, sp).start()
-        return 0
-
-    lax.fori_loop(sp + 1, n_sp, send_state, 0)
-
-    lax.fori_loop(0, chunks - 1, second, 0)
+    keep_all = jnp.broadcast_to(log_half * log_half, (HALO, chans)).astype(BF16)
+    for h in range(heads):
+        lanes = slice(h * DK, (h + 1) * DK)
+        mine_out[h, pl.ds(0, DK), :] = state[:, lanes].astype(BF16)
+        mine_out[h, pl.ds(DK, HALO), :] = keep_all[:, lanes]
+    for step in range(1, row_n):
+        mine_to(lax.rem(x_at + step, row_n), x_at).start()
+    row_in[x_at] = mine_out[x_at]
+
+    with jax.named_scope("L_second"):
+        lax.fori_loop(0, chunks - 1, second, 0)
 
     for i in (3, 4):
         for copy in w_in(i):
@@ -246,12 +288,62 @@
     back = wide_rows - wide_cols
     count = lax.broadcasted_iota(jnp.int32, (BLOCK_ROWS, LANES), 0) + (sp * length + 1)
 
+    def part_of(ref, at):
+        return ref[at, pl.ds(0, DK), :].astype(F32), ref[at, pl.ds(DK, HALO), :].astype(F32)[0:1]
+
+    def fold_row():
+        for step in range(1, row_n):
+            with jax.named_scope("row_recv"):
+                mine_to(x_at, lax.rem(x_at + step, row_n)).wait_recv()
+        total, kept = part_of(row_in, 0)
+        for k in range(1, row_n):
+            term, keep = part_of(row_in, k)
+            total = keep * total + term
+            kept = kept * keep
+        total_out[pl.ds(0, DK), :] = total.astype(BF16)
+        total_out[pl.ds(DK, HALO), :] = jnp.broadcast_to(kept, (HALO, DK)).astype(BF16)
+        each(z_at + 1, col_n, lambda k: total_to(k, z_at).start())
+
+    def fold_column():
+        state[:, pl.ds(0, DK)] = jnp.zeros((DK, DK), F32)
+
+        def take(k):
+            with jax.named_scope("col_recv"):
+                total_to(z_at, k).wait_recv()
+            term, keep = part_of(total_in, k)
+            state[:, pl.ds(0, DK)] = keep * state[:, pl.ds(0, DK)] + term
+
+        each(0, z_at, take)
+        total = state[:, pl.ds(0, DK)]
+        for k in range(row_n):
+            start_out[k] = total.astype(BF16)
+            if k + 1 < row_n:
+                term, keep = part_of(row_in, k)
+                total = keep * total + term
+        for step in range(1, row_n):
+            k = lax.rem(x_at + step, row_n)
+
+            @pl.when(row0 + k > 0)
+            def _():
+                start_to(k, x_at).start()
+
+        start_in[x_at] = start_out[x_at]
+
     def third(step, _):
         c = chunks - 1 - step
 
+        @pl.when(step == 1)
+        def _():
+            fold_row()
+
+        @pl.when(step == chunks - 1)
+        def _():
+            fold_column()
+
         @pl.when((step == chunks - 1) & (sp > 0))
         def _():
-            h_out(sp).wait_recv()
+            with jax.named_scope("halo_recv"):
+                h_out(sp).wait_recv()
             p_buf[pl.ds(BLOCK_ROWS - HALO, HALO), :] = halo_in[...]
 
         rows = pl.ds(pl.multiple_of(c * rows_x, rows_x), rows_x)
@@ -282,7 +374,8 @@
         a_out(0, c).start()
         return 0
 
-    lax.fori_loop(0, chunks, third, 0)
+    with jax.named_scope("L_third"):
+        lax.fori_loop(0, chunks, third, 0)
 
     for i in range(2):
         wo_in(i).wait()
@@ -298,17 +391,25 @@
         r_buf[rows, :] = mine + dot(a_buf[peer, rows, pool_at], wo_buf[peer, pool_at])
         return 0
 
-    lax.fori_loop(0, chunks, pool_part, 0)
-
-    state[...] = jnp.zeros_like(state)
-
-    def join(k, _):
-        st_out(sp, k).wait_recv()
-        keep = state_in[k, pl.ds(DK, HALO), :].astype(F32)[0:1]
-        state[...] = keep * state[...] + state_in[k, pl.ds(0, DK), :].astype(F32)
-        return 0
-
-    lax.fori_loop(0, sp, join, 0)
+    with jax.named_scope("L_pool_part"):
+        lax.fori_loop(0, chunks, pool_part, 0)
+
+    for step in range(1, row_n):
+        k = lax.rem(x_at + step, row_n)
+
+        @pl.when(sp > 0)
+        def _():
+            with jax.named_scope("start_recv"):
+                start_to(x_at, k).wait_recv()
+
+    @pl.when(sp > 0)
+    def _():
+        for h in range(heads):
+            state[:, h * DK:(h + 1) * DK] = start_in[h].astype(F32)
+
+    @pl.when(sp == 0)
+    def _():
+        state[...] = jnp.zeros_like(state)
 
     def fourth(c, _):
         for k in range(per):
@@ -328,7 +429,8 @@
         a_out(1, c).start()
         return 0
 
-    lax.fori_loop(0, chunks, fourth, 0)
+    with jax.named_scope("L_fourth"):
+        lax.fori_loop(0, chunks, fourth, 0)
 
     def fold(x):
         acc = x[:, :LANES]
@@ -352,7 +454,8 @@
         o_out(c).start()
         return 0
 
-    lax.fori_loop(0, chunks, fifth, 0)
+    with jax.named_scope("L_fifth"):
+        lax.fori_loop(0, chunks, fifth, 0)
 
     for c in range(chunks):
         s_out(c).wait_recv()
@@ -369,11 +472,15 @@
     for i in range(2):
         wo_out(i).wait_send()
 
-    def sent_state(k, _):
-        st_out(k, sp).wait_send()
-        return 0
-
-    lax.fori_loop(sp + 1, n_sp, sent_state, 0)
+    for step in range(1, row_n):
+        k = lax.rem(x_at + step, row_n)
+        mine_to(k, x_at).wait_send()
+
+        @pl.when(row0 + k > 0)
+        def _():
+            start_to(k, x_at).wait_send()
+
+    each(z_at + 1, col_n, lambda k: total_to(k, z_at).wait_send())
 
     @pl.when(sp + 1 < n_sp)
     def _():
@@ -425,6 +532,7 @@
               gain, wo_pool, wo_rec, norm_gain, norm_bias):
         length, feats = stream.shape[1], stream.shape[2]
         chans, pool_w = bound.shape[0], scale.shape[0]
+        heads = chans // DK
         blocks = length // BLOCK_ROWS
         rows_x = 256
         chunks = length // rows_x
@@ -446,8 +554,12 @@
             pltpu.VMEM((length, feats), BF16),
             pltpu.VMEM((blocks, 8, chans), F32),
             pltpu.VMEM((DK, chans), F32),
-            pltpu.VMEM((DK + HALO, chans), BF16),
-            pltpu.VMEM((n_sp, DK + HALO, chans), BF16),
+            pltpu.VMEM((heads, DK + HALO, DK), BF16),
+            pltpu.VMEM((heads, DK + HALO, DK), BF16),
+            pltpu.VMEM((DK + HALO, DK), BF16),
+            pltpu.VMEM((n_sp // heads, DK + HALO, DK), BF16),
+            pltpu.VMEM((heads, DK, DK), BF16),
+            pltpu.VMEM((heads, DK, DK), BF16),
             pltpu.VMEM((HALO, pool_w), BF16),
             pltpu.VMEM((chunks, rows_x, LANES), F32),
             pltpu.VMEM((chunks, rows_x, LANES), F32),
@@ -459,7 +571,8 @@
             pltpu.VMEM((1, DK), F32),
             dma((chunks,)), dma((chunks,)), dma((chunks,)), dma((5, n_tp)),
             dma((2,)), dma((2,)), dma((2,)), dma((2, chunks)), dma((2, chunks)),
-            dma((n_sp,)), dma((n_sp,)), dma, dma, dma((chunks,)), dma((chunks,)), dma((chunks,)),
+            dma((heads,)), dma((heads,)), dma((n_sp // heads,)), dma((n_sp // heads,)),
+            dma((heads,)), dma((heads,)), dma, dma, dma((chunks,)), dma((chunks,)), dma((chunks,)),
             dma((chunks,)), dma((5,)),
         ]
         row = lambda x: x.reshape(1, -1)

time: 63.1 us -> 42.4 us (0.67)
  the two profiles are of different devices: /device:TPU:119 before, /device:TPU:1 now
where the time goes in v1:
time: 42.4 us; the launch traced here: 42.3 us
  Pallas kernels  42.3 us (100%)
    pallas_call x1, Pallas kernels, local(): pl.pallas_call(functools.partial(mixer, n_sp, n_tp, rows_x), out_shape=(j...  38.4 us
    pallas_call x1, Pallas kernels, local(): pl.pallas_call(functools.partial(finish, n_tp * feats, piece), out_shape=...  3.84 us

profile of v1, /device:TPU:1, one launch (start us, length us, event | category | flops | bytes accessed | tf_op | source)
XLA Modules:
  0.0 42.3 jit_solution(11068563260316079670)
XLA Ops:
  0.0 38.4 %mixer.1 = (bf16[1024,1024]{1,0:T(8,128)(2,1)}, f32[1024,128]{1,0:T(8,128)}) custom-call(bf16[1,1024,1024]{2,1,0:T(8,128)(2,1)} %stream.1, bf16[2048,512]{1,0:T(8,128)(2,1)} %w_pool.1, bf16[2048,512]{1,0:T(8,128)(2,1)} %w_query.1, bf16[2048,512]{1,0:T(8,128)(2,1)} %w_forget.1, bf16[2048,512]{1,0:T(8,128)(2,1)} %w_value.1, bf16[2048,512]{1,0:T(8,128)(2,1)} %w_gate.1, ...), custom_call_target="tpu_custom_call" | custom-call | tf_op jit(solution)/shard_map/mixer/pallas_call | solution.py:579
  38.4 3.8 %finish.1 = bf16[1,1024,1024]{2,1,0:T(8,128)(2,1)} custom-call(bf16[1024,1024]{1,0:T(8,128)(2,1)} %get-tuple-element.7.resid, f32[1024,128]{1,0:T(8,128)} %get-tuple-element.8.stats, f32[1,1024]{1,0:T(1,128)} %bitcast.7, f32[1,1024]{1,0:T(1,128)} %bitcast.8), custom_call_target="tpu_custom_call" | custom-call | tf_op jit(solution)/shard_map/finish/pallas_call | solution.py:593

commit v2 on v1

v2 whole, which is shorter than its diff:
```python
import functools

import jax
import jax.numpy as jnp
from jax import lax
from jax.experimental import pallas as pl
from jax.experimental.pallas import tpu as pltpu
from jax.sharding import PartitionSpec as P

DK = 128
BLOCK_ROWS = 128
GROUP_CH = 256
HALO = 16
LANES = 128

LIMIT = 56 * 1024 * 1024
ALPHA = 2.0**0.25
EPS_RMS = 1e-06
EPS_NORM = 1e-05
F32 = jnp.float32
BF16 = jnp.bfloat16
NT = (((1,), (1,)), ((), ()))
TN = (((0,), (0,)), ((), ()))
OWN, PEER = 0, 1


def dot(a, b, dims=None):
    if dims is None:
        return jnp.dot(a, b, preferred_element_type=F32)
    return lax.dot_general(a, b, dims, preferred_element_type=F32)


def half_sigmoid(x):
    return 0.5 + 0.5 * jnp.tanh(0.5 * x)


def mixer(
    n_sp, n_tp, rows_x,
    stream, w_pool, w_query, w_forget, w_value, w_gate,
    mix_in, scale_in, bound_in, extra_in, gain_in, wo_pool, wo_rec,
    r_buf, stats,
    x_buf, w_buf, wo_buf, a_buf, v_buf, u_buf, e_buf, t_buf, p_buf, q_buf, g_buf, f_buf,
    half_buf, state, mine_out, row_in, total_out, total_in, start_out, start_in, halo_in,
    stat_own, stat_peer, bands,
    mix, scale, bound, extra, gain,
    x_loc, x_send, x_recv, w_sem, wo_loc, wo_send, wo_recv, a_send, a_recv,
    m_send, m_recv, r_send, r_recv, b_send, b_recv, h_send, h_recv, s_send, s_recv, small_sem,
):
    sp, tp = lax.axis_index("sp"), lax.axis_index("tp")
    peer = 1 - tp
    length, feats = stream.shape[1], stream.shape[2]
    chans = bound.shape[1]
    heads = chans // DK
    pool_w = scale.shape[1]
    groups = mix.shape[0]
    chunks = length // rows_x
    blocks = length // BLOCK_ROWS
    per = rows_x // BLOCK_ROWS
    row_n = heads
    col_n = n_sp // row_n
    x_at, z_at = lax.rem(sp, row_n), lax.div(sp, row_n)
    row0 = z_at * row_n
    mesh_id = pl.DeviceIdType.MESH

    def rows_of(c):
        return slice(c * rows_x, (c + 1) * rows_x)

    def block_of(b):
        return slice(b * BLOCK_ROWS, (b + 1) * BLOCK_ROWS)

    def head_of(h):
        return slice(h * DK, (h + 1) * DK)

    def x_in(c):
        rows = pl.ds(c * rows_x, rows_x)
        return pltpu.make_async_copy(stream.at[0, rows], x_buf.at[OWN, rows], x_loc.at[c])

    def x_out(c):
        rows = pl.ds(c * rows_x, rows_x)
        return pltpu.make_async_remote_copy(
            x_buf.at[OWN, rows], x_buf.at[PEER, rows], x_send.at[c], x_recv.at[c],
            device_id={"tp": peer}, device_id_type=mesh_id)

    my_cols = pl.ds(pl.multiple_of(tp * feats, LANES), feats)
    peer_cols = pl.ds(pl.multiple_of(peer * feats, LANES), feats)
    wo_places = ((wo_pool, pl.ds(0, pool_w)), (wo_rec, pl.ds(pool_w, chans)))

    def w_in(i, side):
        src = (w_forget, w_value, w_pool, w_query, w_gate)[i]
        return pltpu.make_async_copy(
            src.at[my_cols if side == OWN else peer_cols], w_buf.at[i, side], w_sem.at[i, side])

    def wo_in(i):
        src, place = wo_places[i]
        return pltpu.make_async_copy(src.at[:, my_cols], wo_buf.at[OWN, place], wo_loc.at[i])

    def wo_out(i):
        src, place = wo_places[i]
        return pltpu.make_async_remote_copy(
            src.at[:, peer_cols], wo_buf.at[PEER, place], wo_send.at[i], wo_recv.at[i],
            device_id={"tp": peer}, device_id_type=mesh_id)

    def a_out(i, c):
        rows, cols = pl.ds(c * rows_x, rows_x), wo_places[i][1]
        return pltpu.make_async_remote_copy(
            a_buf.at[OWN, rows, cols], a_buf.at[PEER, rows, cols], a_send.at[i, c], a_recv.at[i, c],
            device_id={"tp": peer}, device_id_type=mesh_id)

    def mine_to(k, slot):
        return pltpu.make_async_remote_copy(
            mine_out.at[k], row_in.at[slot], m_send.at[k], m_recv.at[slot],
            device_id={"sp": row0 + k}, device_id_type=mesh_id)

    def total_to(k, slot):
        return pltpu.make_async_remote_copy(
            total_out, total_in.at[slot], r_send.at[k], r_recv.at[slot],
            device_id={"sp": k * row_n + x_at}, device_id_type=mesh_id)

    def start_to(k, slot):
        return pltpu.make_async_remote_copy(
            start_out.at[k], start_in.at[slot], b_send.at[k], b_recv.at[slot],
            device_id={"sp": row0 + k}, device_id_type=mesh_id)

    def h_out(k):
        return pltpu.make_async_remote_copy(
            p_buf.at[pl.ds(BLOCK_ROWS + length - HALO, HALO)], halo_in, h_send, h_recv,
            device_id={"sp": k}, device_id_type=mesh_id)

    def s_out(c):
        return pltpu.make_async_remote_copy(
            stat_own.at[c], stat_peer.at[c], s_send.at[c], s_recv.at[c],
            device_id={"tp": peer}, device_id_type=mesh_id)

    def greet(k):
        pl.semaphore_signal(barrier, inc=1, device_id={"sp": k}, device_id_type=mesh_id)

    def each(low, high, do):
        def step(k, _):
            do(k)
            return 0

        lax.fori_loop(low, high, step, 0)

    smalls = [
        pltpu.make_async_copy(src, dst, small_sem.at[i])
        for i, (src, dst) in enumerate(
            ((extra_in, extra), (bound_in, bound), (mix_in, mix), (scale_in, scale), (gain_in, gain)))
    ]

    smalls[0].start()
    x_in(0).start()
    w_in(0, OWN).start()
    w_in(1, OWN).start()
    for c in range(1, chunks):
        x_in(c).start()
    w_in(0, PEER).start()
    w_in(1, PEER).start()
    for copy in smalls[1:]:
        copy.start()

    barrier = pltpu.get_barrier_semaphore()
    pl.semaphore_signal(barrier, inc=1, device_id={"tp": peer}, device_id_type=mesh_id)
    p_buf[0:BLOCK_ROWS, :] = jnp.zeros((BLOCK_ROWS, pool_w), BF16)
    with jax.named_scope("entry"):
        pl.semaphore_wait(barrier, 1 + x_at + z_at)
    for step in range(1, row_n):
        greet(row0 + lax.rem(x_at + step, row_n))
    for step in range(1, col_n):
        greet(lax.rem(z_at + step, col_n) * row_n + x_at)
    leads = (x_at == 0) & (z_at > 0)
    ends = (x_at == row_n - 1) & (z_at < col_n - 1)
    later = (row_n - 1 - x_at) + (col_n - 1 - z_at) + jnp.where(ends, 1, 0)

    with jax.named_scope("x0"):
        x_in(0).wait()
        x_out(0).start()
        smalls[0].wait()

    row_ids = lax.broadcasted_iota(jnp.int32, (BLOCK_ROWS, BLOCK_ROWS), 0)
    col_ids = lax.broadcasted_iota(jnp.int32, (BLOCK_ROWS, BLOCK_ROWS), 1)
    lower = row_ids >= col_ids

    with jax.named_scope("drops"):
        lower_twice = jnp.concatenate([row_ids, row_ids], axis=1) >= jnp.concatenate([col_ids, col_ids], axis=1)
        ones = jnp.ones((2 * BLOCK_ROWS, DK), BF16)
        for b in range(blocks):
            drop = extra[:, block_of(b)]
            drop_high = drop.astype(BF16).astype(F32)
            drop_low = drop - drop_high
            for h in range(heads):
                pair = jnp.concatenate([drop_high[h:h + 1], drop_low[h:h + 1]], axis=1)
                wide = jnp.where(lower_twice, jnp.broadcast_to(pair, (BLOCK_ROWS, 2 * BLOCK_ROWS)), 0.0)
                e_buf[block_of(b), head_of(h)] = dot(wide.astype(BF16), ones)
        wide_rows = lax.broadcasted_iota(jnp.int32, (BLOCK_ROWS, 2 * BLOCK_ROWS), 0) + BLOCK_ROWS
        wide_cols = lax.broadcasted_iota(jnp.int32, (BLOCK_ROWS, 2 * BLOCK_ROWS), 1)
        back = wide_rows - wide_cols
        for j in range(groups):
            window = jnp.left_shift(jnp.int32(2), tp * groups + j)
            share = 1.0 / window.astype(F32)
            inside = (back >= 0) & (back < window)
            bands[j] = (jnp.where(inside, share, 0.0) - jnp.where(back == 0, 1.0, 0.0)).astype(BF16)
        state[...] = jnp.zeros_like(state)

    with jax.named_scope("x_rest"):
        for c in range(1, chunks):
            x_in(c).wait()
            x_out(c).start()
    with jax.named_scope("w01"):
        for i in (0, 1):
            w_in(i, OWN).wait()

    tri = jnp.where(lower, 1.0, 0.0).astype(BF16)
    tri_twice = jnp.concatenate([tri, tri], axis=1)

    def proj(i, c):
        rows = rows_of(c)
        return dot(x_buf[OWN, rows, :], w_buf[i, OWN]) + dot(x_buf[PEER, rows, :], w_buf[i, PEER])

    class Post:
        def __init__(self, c):
            self.blocks = [c * per + j for j in range(per)]
            self.weight, self.split, self.total = {}, {}, {}
            self.down, self.half = {}, {}

        def logs(self):
            open_part = 1.0 - bound[...]
            for b in self.blocks:
                f_in = f_buf[block_of(b), :].astype(F32)
                weight = open_part * (0.5 - 0.5 * jnp.tanh(0.5 * f_in))
                keep = jnp.log(1.0 - weight)
                high = keep.astype(BF16)
                low = (keep - high.astype(F32)).astype(BF16)
                self.weight[b], self.split[b] = weight, jnp.concatenate([high, low], axis=0)

        def sums(self):
            for b in self.blocks:
                self.total[b] = dot(tri_twice, self.split[b]) + e_buf[block_of(b), :]

        def exps(self):
            for b in self.blocks:
                total = self.total[b]
                middle = 0.5 * total[BLOCK_ROWS - 1:BLOCK_ROWS]
                e_buf[block_of(b), :] = jnp.exp(total - middle)
                down = (self.weight[b] * jnp.exp(middle - total)).astype(BF16)
                u_buf[block_of(b), :] = down
                half = jnp.exp(middle)
                half_buf[b] = jnp.broadcast_to(half, (8, chans))
                self.down[b], self.half[b] = down, half

        def states(self):
            for b in self.blocks:
                for h in range(heads):
                    lanes = head_of(h)
                    hh = self.half[b][:, lanes]
                    term = dot(v_buf[block_of(b), lanes], self.down[b][:, lanes], TN) * hh
                    t_buf[b, :, lanes] = term
                    state[:, lanes] = hh * hh * state[:, lanes] + term

    def put_pool(c):
        p_buf[BLOCK_ROWS + c * rows_x:BLOCK_ROWS + (c + 1) * rows_x, :] = proj(2, c).astype(BF16)

    with jax.named_scope("first0"):
        own = x_buf[OWN, rows_of(0), :]
        f_own = dot(own, w_buf[0, OWN])
        v_own = dot(own, w_buf[1, OWN])
        with jax.named_scope("x_recv0"):
            x_out(0).wait_recv()
            for i in (0, 1):
                w_in(i, PEER).wait()
            for copy in smalls[1:]:
                copy.wait()
        for i in (2, 3, 4):
            for side in (OWN, PEER):
                w_in(i, side).start()
        for i in range(2):
            wo_in(i).start()
            wo_out(i).start()
        other = x_buf[PEER, rows_of(0), :]
        f_buf[rows_of(0), :] = (f_own + dot(other, w_buf[0, PEER])).astype(BF16)
        v_buf[rows_of(0), :] = (v_own + dot(other, w_buf[1, PEER])).astype(BF16)

    for c in range(1, chunks):
        with jax.named_scope("first"):
            with jax.named_scope("x_recv"):
                x_out(c).wait_recv()
            if c == 2:
                @pl.when(leads)
                def _():
                    with jax.named_scope("lead"):
                        pl.semaphore_wait(barrier, later)
                    greet(sp - 1)
            post = Post(c - 1)
            post.logs()
            f_buf[rows_of(c), :] = proj(0, c).astype(BF16)
            post.sums()
            v_buf[rows_of(c), :] = proj(1, c).astype(BF16)
            post.exps()
            post.states()

    with jax.named_scope("w2"):
        for side in (OWN, PEER):
            w_in(2, side).wait()
    with jax.named_scope("second0"):
        post = Post(chunks - 1)
        post.logs()
        put_pool(chunks - 1)
        post.sums()
        put_pool(chunks - 2)
        post.exps()
        post.states()
        log_half = half_buf[0, 0:1]
        for b in range(1, blocks):
            log_half = log_half * half_buf[b, 0:1]
        keep_all = jnp.broadcast_to(log_half * log_half, (HALO, chans)).astype(BF16)
        for h in range(heads):
            mine_out[h, 0:DK, :] = state[:, head_of(h)].astype(BF16)
            mine_out[h, DK:DK + HALO, :] = keep_all[:, head_of(h)]

    @pl.when(jnp.logical_not(leads) & (sp + 1 < n_sp))
    def _():
        with jax.named_scope("later"):
            pl.semaphore_wait(barrier, later)

    for step in range(1, row_n):
        mine_to(lax.rem(x_at + step, row_n), x_at).start()
    row_in[x_at] = mine_out[x_at]

    @pl.when(sp + 1 < n_sp)
    def _():
        h_out(sp + 1).start()

    with jax.named_scope("second"):
        for c in range(chunks - 2):
            put_pool(c)

    with jax.named_scope("w34"):
        for i in (3, 4):
            for side in (OWN, PEER):
                w_in(i, side).wait()

    def part_of(ref, at):
        return ref[at, 0:DK, :].astype(F32), ref[at, DK:DK + HALO, :].astype(F32)[0:1]

    def fold_row():
        for step in range(1, row_n):
            with jax.named_scope("row_recv"):
                mine_to(x_at, lax.rem(x_at + step, row_n)).wait_recv()
        total, kept = part_of(row_in, 0)
        for k in range(1, row_n):
            term, keep = part_of(row_in, k)
            total = keep * total + term
            kept = kept * keep
        total_out[0:DK, :] = total.astype(BF16)
        total_out[DK:DK + HALO, :] = jnp.broadcast_to(kept, (HALO, DK)).astype(BF16)
        each(z_at + 1, col_n, lambda k: total_to(k, z_at).start())

    def fold_column():
        state[:, 0:DK] = jnp.zeros((DK, DK), F32)

        def take(k):
            with jax.named_scope("col_recv"):
                total_to(z_at, k).wait_recv()
            term, keep = part_of(total_in, k)
            state[:, 0:DK] = keep * state[:, 0:DK] + term

        each(0, z_at, take)
        total = state[:, 0:DK]
        for k in range(row_n):
            start_out[k] = total.astype(BF16)
            if k + 1 < row_n:
                term, keep = part_of(row_in, k)
                total = keep * total + term
        for step in range(1, row_n):
            k = lax.rem(x_at + step, row_n)

            @pl.when(row0 + k > 0)
            def _():
                start_to(k, x_at).start()

        start_in[x_at] = start_out[x_at]

    count = lax.broadcasted_iota(jnp.int32, (BLOCK_ROWS, LANES), 0) + (sp * length + 1)

    class Third:
        def __init__(self, c):
            self.c, self.rows = c, rows_of(c)
            self.blocks = [c * per + k for k in range(per)]
            self.diff, self.scores = {}, {}

        def query(self):
            q_in = proj(3, self.c).astype(BF16).astype(F32)
            q_buf[self.rows, :] = (q_in * half_sigmoid(q_in) * e_buf[self.rows, :]).astype(BF16)

        def band(self):
            for b in self.blocks:
                near = p_buf[b * BLOCK_ROWS:(b + 2) * BLOCK_ROWS, :]
                for j in range(groups):
                    lanes = slice(j * GROUP_CH, (j + 1) * GROUP_CH)
                    if b:
                        self.diff[b, j] = dot(bands[j], near[:, lanes]).astype(BF16)
                        continue
                    window = jnp.left_shift(jnp.int32(2), tp * groups + j)
                    inside = jnp.where((back >= 0) & (back < window), 1.0, 0.0).astype(BF16)
                    share = 1.0 / jnp.minimum(count, window).astype(F32)
                    share = jnp.concatenate([share] * (GROUP_CH // LANES), axis=1)
                    sums = dot(inside, near[:, lanes])
                    self.diff[b, j] = (sums * share - near[BLOCK_ROWS:, lanes].astype(F32)).astype(BF16)

        def gates(self):
            g_buf[self.rows, :] = proj(4, self.c).astype(BF16)

        def mixed(self):
            for b in self.blocks:
                for j in range(groups):
                    lanes = slice(j * GROUP_CH, (j + 1) * GROUP_CH)
                    a_buf[OWN, block_of(b), lanes] = (dot(self.diff[b, j], mix[j]) * scale[:, lanes]).astype(BF16)

        def score(self):
            for b in self.blocks:
                for h in range(heads):
                    up, down = q_buf[block_of(b), head_of(h)], u_buf[block_of(b), head_of(h)]
                    self.scores[b, h] = jnp.where(lower, dot(up, down, NT), 0.0).astype(BF16)

        def inner(self):
            for b in self.blocks:
                for h in range(heads):
                    e_buf[block_of(b), head_of(h)] = dot(self.scores[b, h], v_buf[block_of(b), head_of(h)])

    for c in reversed(range(chunks)):
        if c == 1:
            fold_row()
        if c == 0:
            fold_column()

            @pl.when(sp > 0)
            def _():
                with jax.named_scope("halo_recv"):
                    h_out(sp).wait_recv()
                p_buf[BLOCK_ROWS - HALO:BLOCK_ROWS, :] = halo_in[...]

        with jax.named_scope("third"):
            part = Third(c)
            part.query()
            part.band()
            part.gates()
            part.mixed()
            part.score()
            part.inner()
            a_out(0, c).start()

    with jax.named_scope("wo"):
        for i in range(2):
            wo_in(i).wait()
            wo_out(i).wait_recv()

    pool_at, rec_at = slice(0, pool_w), slice(pool_w, pool_w + chans)

    def pool_part(c):
        rows = rows_of(c)
        r_buf[rows, :] = (
            dot(a_buf[OWN, rows, pool_at], wo_buf[OWN, pool_at]) + dot(a_buf[PEER, rows, pool_at], wo_buf[PEER, pool_at])
            + ALPHA * x_buf[OWN, rows, :].astype(F32))

    with jax.named_scope("pool"):
        for c in reversed(range(2, chunks)):
            a_out(0, c).wait_recv()
        for c in reversed(range(2, chunks)):
            pool_part(c)

    for step in range(1, row_n):
        k = lax.rem(x_at + step, row_n)

        @pl.when(sp > 0)
        def _():
            with jax.named_scope("start_recv"):
                start_to(x_at, k).wait_recv()

    @pl.when(sp > 0)
    def _():
        for h in range(heads):
            state[:, head_of(h)] = start_in[h].astype(F32)

    @pl.when(sp == 0)
    def _():
        state[...] = jnp.zeros_like(state)

    def fourth(c):
        for k in range(per):
            b = c * per + k
            half = half_buf[b, 0:1]
            before = state[...] * half
            carried = before.astype(BF16)
            state[...] = before * half + t_buf[b]
            for h in range(heads):
                lanes = head_of(h)
                raw = e_buf[block_of(b), lanes] + dot(q_buf[block_of(b), lanes], carried[:, lanes], NT)
                power = jnp.mean(raw * raw, axis=-1, keepdims=True)
                gate = g_buf[block_of(b), lanes].astype(F32)
                rec = raw * lax.rsqrt(power + EPS_RMS) * gain[...] * (gate * half_sigmoid(gate))
                a_buf[OWN, block_of(b), pool_w + h * DK:pool_w + (h + 1) * DK] = rec.astype(BF16)

    for c in range(chunks):
        with jax.named_scope("fourth"):
            fourth(c)
            if c < 2:
                a_out(0, 1 - c).wait_recv()
                pool_part(1 - c)
            a_out(1, c).start()

    def fold(x):
        acc = x[:, :LANES]
        for k in range(1, feats // LANES):
            acc = acc + x[:, k * LANES:(k + 1) * LANES]
        return acc

    first_half = lax.broadcasted_iota(jnp.int32, (rows_x, LANES), 1) < LANES // 2

    for c in range(chunks):
        with jax.named_scope("fifth"):
            rows = rows_of(c)
            a_out(1, c).wait_recv()
            resid = r_buf[rows, :] + (
                dot(a_buf[OWN, rows, rec_at], wo_buf[OWN, rec_at]) + dot(a_buf[PEER, rows, rec_at], wo_buf[PEER, rec_at]))
            r_buf[rows, :] = resid
            sums, squares = fold(resid), fold(resid * resid)
            sums = sums + pltpu.roll(sums, LANES // 2, 1)
            squares = squares + pltpu.roll(squares, LANES // 2, 1)
            stat_own[c] = jnp.where(first_half, sums, squares)
            s_out(c).start()

    with jax.named_scope("tail"):
        for c in range(chunks):
            s_out(c).wait_recv()
            stats[rows_of(c), :] = stat_own[c] + stat_peer[c]

        for c in range(chunks):
            x_out(c).wait_send()
            s_out(c).wait_send()
            for i in range(2):
                a_out(i, c).wait_send()
        for i in range(2):
            wo_out(i).wait_send()
        for step in range(1, row_n):
            k = lax.rem(x_at + step, row_n)
            mine_to(k, x_at).wait_send()

            @pl.when(row0 + k > 0)
            def _():
                start_to(k, x_at).wait_send()

        each(z_at + 1, col_n, lambda k: total_to(k, z_at).wait_send())

        @pl.when(sp + 1 < n_sp)
        def _():
            h_out(sp + 1).wait_send()


def finish(width, rows, resid, stats, gain, bias, out, o_buf, o_sem):
    pieces = resid.shape[0] // rows

    def leave(c):
        part = pl.ds(c * rows, rows)
        return pltpu.make_async_copy(o_buf.at[part], out.at[0, part], o_sem.at[c])

    first_half = lax.broadcasted_iota(jnp.int32, (rows, LANES), 1) < LANES // 2
    for c in range(pieces):
        part = slice(c * rows, (c + 1) * rows)
        both = stats[part, :]
        mean = jnp.sum(jnp.where(first_half, both, 0.0), axis=1, keepdims=True) / width
        square = jnp.sum(jnp.where(first_half, 0.0, both), axis=1, keepdims=True) / width
        inv = lax.rsqrt(square - mean * mean + EPS_NORM)
        o_buf[part, :] = ((resid[part, :] - mean) * inv * gain[...] + bias[...]).astype(BF16)
        leave(c).start()
    for c in range(pieces):
        leave(c).wait()


def solution(mesh):
    n_sp, n_tp = mesh.shape["sp"], mesh.shape["tp"]

    def local(stream, w_pool, w_query, w_forget, w_value, w_gate, mix, scale, bound, extra,
              gain, wo_pool, wo_rec, norm_gain, norm_bias):
        length, feats = stream.shape[1], stream.shape[2]
        chans, pool_w = bound.shape[0], scale.shape[0]
        heads = chans // DK
        blocks = length // BLOCK_ROWS
        rows_x = 256
        chunks = length // rows_x
        hbm = pl.BlockSpec(memory_space=pl.ANY)
        vmem = pl.BlockSpec(memory_space=pltpu.VMEM)
        dma = pltpu.SemaphoreType.DMA
        scratch = [
            pltpu.VMEM((n_tp, length, feats), BF16),
            pltpu.VMEM((5, n_tp, feats, chans), BF16),
            pltpu.VMEM((n_tp, pool_w + chans, feats), BF16),
            pltpu.VMEM((n_tp, length, pool_w + chans), BF16),
            pltpu.VMEM((length, chans), BF16),
            pltpu.VMEM((length, chans), BF16),
            pltpu.VMEM((length, chans), F32),
            pltpu.VMEM((blocks, DK, chans), F32),
            pltpu.VMEM((BLOCK_ROWS + length, pool_w), BF16),
            pltpu.VMEM((length, chans), BF16),
            pltpu.VMEM((length, chans), BF16),
            pltpu.VMEM((length, chans), BF16),
            pltpu.VMEM((blocks, 8, chans), F32),
            pltpu.VMEM((DK, chans), F32),
            pltpu.VMEM((heads, DK + HALO, DK), BF16),
            pltpu.VMEM((heads, DK + HALO, DK), BF16),
            pltpu.VMEM((DK + HALO, DK), BF16),
            pltpu.VMEM((n_sp // heads, DK + HALO, DK), BF16),
            pltpu.VMEM((heads, DK, DK), BF16),
            pltpu.VMEM((heads, DK, DK), BF16),
            pltpu.VMEM((HALO, pool_w), BF16),
            pltpu.VMEM((chunks, rows_x, LANES), F32),
            pltpu.VMEM((chunks, rows_x, LANES), F32),
            pltpu.VMEM((mix.shape[0], BLOCK_ROWS, 2 * BLOCK_ROWS), BF16),
            pltpu.VMEM(mix.shape, BF16),
            pltpu.VMEM((1, pool_w), F32),
            pltpu.VMEM((1, chans), F32),
            pltpu.VMEM((heads, length), F32),
            pltpu.VMEM((1, DK), F32),
            dma((chunks,)), dma((chunks,)), dma((chunks,)), dma((5, n_tp)),
            dma((2,)), dma((2,)), dma((2,)), dma((2, chunks)), dma((2, chunks)),
            dma((heads,)), dma((heads,)), dma((n_sp // heads,)), dma((n_sp // heads,)),
            dma((heads,)), dma((heads,)), dma, dma, dma((chunks,)), dma((chunks,)), dma((5,)),
        ]
        row = lambda x: x.reshape(1, -1)
        resid, stats = pl.pallas_call(
            functools.partial(mixer, n_sp, n_tp, rows_x),
            out_shape=(pltpu.VMEM((length, feats), F32), pltpu.VMEM((length, LANES), F32)),
            in_specs=[hbm] * 13,
            out_specs=(vmem, vmem),
            scratch_shapes=scratch,
            compiler_params=pltpu.CompilerParams(
                collective_id=0, has_side_effects=True, vmem_limit_bytes=LIMIT),
            name="mixer",
        )(stream, w_pool, w_query, w_forget, w_value, w_gate, mix, row(scale), row(bound), extra.T,
          row(gain), wo_pool, wo_rec)
        piece = 128
        pieces = length // piece
        return pl.pallas_call(
            functools.partial(finish, n_tp * feats, piece),
            out_shape=jax.ShapeDtypeStruct(stream.shape, BF16),
            in_specs=[vmem] * 4,
            out_specs=hbm,
            scratch_shapes=[pltpu.VMEM((length, feats), BF16), dma((pieces,))],
            compiler_params=pltpu.CompilerParams(vmem_limit_bytes=16 * 1024 * 1024),
            name="finish",
        )(resid, stats, row(norm_gain), row(norm_bias))

    placed = (
        P("fs", "sp", "tp"), P(None, "tp"), P(None, "tp"), P(None, "tp"), P(None, "tp"),
        P(None, "tp"), P("tp", None, None), P("tp"), P("tp"), P("sp", "tp"), P(),
        P("tp", None), P("tp", None), P("tp"), P("tp"),
    )
    return jax.shard_map(
        local, mesh=mesh, in_specs=placed, out_specs=P("fs", "sp", "tp"), check_vma=False
    )
```

time: 42.4 us -> 34.6 us (0.82)
  the two profiles are of different devices: /device:TPU:1 before, /device:TPU:81 now
where the time goes in v2:
time: 34.6 us; the launch traced here: 34.5 us
  Pallas kernels  34.3 us (99%)
    pallas_call x1, Pallas kernels, local(): pl.pallas_call(functools.partial(mixer, n_sp, n_tp, rows_x), out_shape=(p...  32.4 us
    pallas_call x1, Pallas kernels, local(): pl.pallas_call(functools.partial(finish, n_tp * feats, piece), out_shape=...  1.85 us

profile of v2, /device:TPU:81, one launch (start us, length us, event | category | flops | bytes accessed | tf_op | source)
XLA Modules:
  0.0 34.5 jit_solution(8067439704201611245)
XLA Ops:
  0.0 0.0 copy-start
  0.0 0.0 copy-start.1
  0.0 32.4 %mixer.1 = (f32[1024,1024]{1,0:T(8,128)S(1)}, f32[1024,128]{1,0:T(8,128)S(1)}) custom-call(bf16[1,1024,1024]{2,1,0:T(8,128)(2,1)} %stream.1, bf16[2048,512]{1,0:T(8,128)(2,1)} %w_pool.1, bf16[2048,512]{1,0:T(8,128)(2,1)} %w_query.1, bf16[2048,512]{1,0:T(8,128)(2,1)} %w_forget.1, bf16[2048,512]{1,0:T(8,128)(2,1)} %w_value.1, bf16[2048,512]{1,0:T(8,128)(2,1)} %w_gate.1, ...), custom_call_target="tpu_custom_call" | custom-call | tf_op jit(solution)/shard_map/mixer/pallas_call | solution.py:628
  32.4 0.0 copy-done
  32.5 0.0 copy-done.1
  32.5 1.8 %finish.1 = bf16[1,1024,1024]{2,1,0:T(8,128)(2,1)} custom-call(f32[1024,1024]{1,0:T(8,128)S(1)} %get-tuple-element.7.resid, f32[1024,128]{1,0:T(8,128)S(1)} %get-tuple-element.8.stats, f32[1,1024]{1,0:T(1,128)S(1)} %bitcast.6, f32[1,1024]{1,0:T(1,128)S(1)} %bitcast.7), custom_call_target="tpu_custom_call" | custom-call | tf_op jit(solution)/shard_map/finish/pallas_call | solution.py:641
Async XLA Ops:
  0.0 32.4 %copy-start = (f32[1024]{0:T(1024)S(1)}, f32[1024]{0:T(1024)}, u32[]{:S(2)}) copy-start(f32[1024]{0:T(1024)} %param.28) | copy-start | bytes 12292
  0.0 32.5 %copy-start.1 = (f32[1024]{0:T(1024)S(1)}, f32[1024]{0:T(1024)}, u32[]{:S(2)}) copy-start(f32[1024]{0:T(1024)} %param.29) | copy-start | bytes 12292

commit v3 on v2

--- a/solution.py
+++ b/solution.py
@@ -44,7 +44,7 @@
     stat_own, stat_peer, bands,
     mix, scale, bound, extra, gain,
     x_loc, x_send, x_recv, w_sem, wo_loc, wo_send, wo_recv, a_send, a_recv,
-    m_send, m_recv, r_send, r_recv, b_send, b_recv, h_send, h_recv, s_send, s_recv, small_sem,
+    m_send, m_recv, r_send, r_recv, b_send, b_recv, h_send, h_recv, s_send, s_recv, small_sem, ready,
 ):
     sp, tp = lax.axis_index("sp"), lax.axis_index("tp")
     peer = 1 - tp
@@ -71,68 +71,84 @@
     def head_of(h):
         return slice(h * DK, (h + 1) * DK)
 
-    def x_in(c):
-        rows = pl.ds(c * rows_x, rows_x)
-        return pltpu.make_async_copy(stream.at[0, rows], x_buf.at[OWN, rows], x_loc.at[c])
-
-    def x_out(c):
-        rows = pl.ds(c * rows_x, rows_x)
+    x_pieces = ((0, rows_x), (rows_x, rows_x), (2 * rows_x, length - 2 * rows_x))
+    pool_pieces = ((length // 2, length // 2), (0, length // 2))
+    rec_pieces = ((0, 2 * rows_x),) + tuple((c * rows_x, rows_x) for c in range(2, chunks))
+    stat_pieces = ((0, length // 2), (length // 2, length // 2))
+
+    def to_peer(src, dst, send, recv):
         return pltpu.make_async_remote_copy(
-            x_buf.at[OWN, rows], x_buf.at[PEER, rows], x_send.at[c], x_recv.at[c],
-            device_id={"tp": peer}, device_id_type=mesh_id)
+            src, dst, send, recv, device_id={"tp": peer}, device_id_type=mesh_id)
+
+    def to_sp(src, dst, send, recv, k):
+        return pltpu.make_async_remote_copy(
+            src, dst, send, recv, device_id={"sp": k}, device_id_type=mesh_id)
+
+    def x_in(i):
+        rows = pl.ds(*x_pieces[i])
+        return pltpu.make_async_copy(stream.at[0, rows], x_buf.at[OWN, rows], x_loc.at[i])
+
+    def x_out(i):
+        rows = pl.ds(*x_pieces[i])
+        return to_peer(x_buf.at[OWN, rows], x_buf.at[PEER, rows], x_send, x_recv.at[i])
 
     my_cols = pl.ds(pl.multiple_of(tp * feats, LANES), feats)
     peer_cols = pl.ds(pl.multiple_of(peer * feats, LANES), feats)
     wo_places = ((wo_pool, pl.ds(0, pool_w)), (wo_rec, pl.ds(pool_w, chans)))
 
+    w_groups = {(0, OWN): 0, (1, OWN): 1, (0, PEER): 2, (1, PEER): 2, (2, OWN): 3, (2, PEER): 3}
+
     def w_in(i, side):
         src = (w_forget, w_value, w_pool, w_query, w_gate)[i]
         return pltpu.make_async_copy(
-            src.at[my_cols if side == OWN else peer_cols], w_buf.at[i, side], w_sem.at[i, side])
+            src.at[my_cols if side == OWN else peer_cols], w_buf.at[i, side], w_sem.at[w_groups.get((i, side), 4)])
+
+    def w_wait(ref, group):
+        pltpu.make_async_copy(ref, ref, w_sem.at[group]).wait()
 
     def wo_in(i):
         src, place = wo_places[i]
-        return pltpu.make_async_copy(src.at[:, my_cols], wo_buf.at[OWN, place], wo_loc.at[i])
+        return pltpu.make_async_copy(src.at[:, my_cols], wo_buf.at[OWN, place], wo_loc)
 
     def wo_out(i):
         src, place = wo_places[i]
-        return pltpu.make_async_remote_copy(
-            src.at[:, peer_cols], wo_buf.at[PEER, place], wo_send.at[i], wo_recv.at[i],
-            device_id={"tp": peer}, device_id_type=mesh_id)
-
-    def a_out(i, c):
-        rows, cols = pl.ds(c * rows_x, rows_x), wo_places[i][1]
-        return pltpu.make_async_remote_copy(
-            a_buf.at[OWN, rows, cols], a_buf.at[PEER, rows, cols], a_send.at[i, c], a_recv.at[i, c],
-            device_id={"tp": peer}, device_id_type=mesh_id)
+        return to_peer(src.at[:, peer_cols], wo_buf.at[PEER, place], wo_send, wo_recv)
+
+    def pool_out(i):
+        rows, cols = pl.ds(*pool_pieces[i]), wo_places[0][1]
+        return to_peer(a_buf.at[OWN, rows, cols], a_buf.at[PEER, rows, cols], a_send, a_recv.at[i])
+
+    def rec_out(i):
+        rows, cols = pl.ds(*rec_pieces[i]), wo_places[1][1]
+        return to_peer(a_buf.at[OWN, rows, cols], a_buf.at[PEER, rows, cols], a_send, a_recv.at[len(pool_pieces) + i])
 
     def mine_to(k, slot):
-        return pltpu.make_async_remote_copy(
-            mine_out.at[k], row_in.at[slot], m_send.at[k], m_recv.at[slot],
-            device_id={"sp": row0 + k}, device_id_type=mesh_id)
+        return to_sp(mine_out.at[k], row_in.at[slot], m_send, m_recv, row0 + k)
 
     def total_to(k, slot):
-        return pltpu.make_async_remote_copy(
-            total_out, total_in.at[slot], r_send.at[k], r_recv.at[slot],
-            device_id={"sp": k * row_n + x_at}, device_id_type=mesh_id)
+        return to_sp(total_out, total_in.at[slot], r_send, r_recv, k * row_n + x_at)
 
     def start_to(k, slot):
-        return pltpu.make_async_remote_copy(
-            start_out.at[k], start_in.at[slot], b_send.at[k], b_recv.at[slot],
-            device_id={"sp": row0 + k}, device_id_type=mesh_id)
+        return to_sp(start_out.at[k], start_in.at[slot], b_send, b_recv, row0 + k)
+
+    def some(ref, count, send, recv):
+        return to_sp(ref.at[0:count], ref.at[0:count], send, recv, row0)
+
+    def when_equal(value, counts, do):
+        for n in counts:
+            @pl.when(value == n)
+            def _():
+                do(n)
 
     def h_out(k):
-        return pltpu.make_async_remote_copy(
-            p_buf.at[pl.ds(BLOCK_ROWS + length - HALO, HALO)], halo_in, h_send, h_recv,
-            device_id={"sp": k}, device_id_type=mesh_id)
-
-    def s_out(c):
-        return pltpu.make_async_remote_copy(
-            stat_own.at[c], stat_peer.at[c], s_send.at[c], s_recv.at[c],
-            device_id={"tp": peer}, device_id_type=mesh_id)
+        return to_sp(p_buf.at[pl.ds(BLOCK_ROWS + length - HALO, HALO)], halo_in, h_send, h_recv, k)
+
+    def s_out(i):
+        rows = pl.ds(*stat_pieces[i])
+        return to_peer(stat_own.at[rows], stat_peer.at[rows], s_send, s_recv.at[i])
 
     def greet(k):
-        pl.semaphore_signal(barrier, inc=1, device_id={"sp": k}, device_id_type=mesh_id)
+        pl.semaphore_signal(ready, inc=1, device_id={"sp": k}, device_id_type=mesh_id)
 
     def each(low, high, do):
         def step(k, _):
@@ -149,10 +165,10 @@
 
     smalls[0].start()
     x_in(0).start()
+    x_in(1).start()
     w_in(0, OWN).start()
     w_in(1, OWN).start()
-    for c in range(1, chunks):
-        x_in(c).start()
+    x_in(2).start()
     w_in(0, PEER).start()
     w_in(1, PEER).start()
     for copy in smalls[1:]:
@@ -160,20 +176,17 @@
 
     barrier = pltpu.get_barrier_semaphore()
     pl.semaphore_signal(barrier, inc=1, device_id={"tp": peer}, device_id_type=mesh_id)
-    p_buf[0:BLOCK_ROWS, :] = jnp.zeros((BLOCK_ROWS, pool_w), BF16)
-    with jax.named_scope("entry"):
-        pl.semaphore_wait(barrier, 1 + x_at + z_at)
-    for step in range(1, row_n):
-        greet(row0 + lax.rem(x_at + step, row_n))
-    for step in range(1, col_n):
-        greet(lax.rem(z_at + step, col_n) * row_n + x_at)
+
+    def hail(k):
+        pl.semaphore_signal(barrier, inc=1, device_id={"sp": k}, device_id_type=mesh_id)
+
+    each(x_at + 1, row_n, lambda k: hail(row0 + k))
+    each(z_at + 1, col_n, lambda k: hail(k * row_n + x_at))
     leads = (x_at == 0) & (z_at > 0)
     ends = (x_at == row_n - 1) & (z_at < col_n - 1)
     later = (row_n - 1 - x_at) + (col_n - 1 - z_at) + jnp.where(ends, 1, 0)
-
-    with jax.named_scope("x0"):
-        x_in(0).wait()
-        x_out(0).start()
+    p_buf[0:BLOCK_ROWS, :] = jnp.zeros((BLOCK_ROWS, pool_w), BF16)
+    with jax.named_scope("extra"):
         smalls[0].wait()
 
     row_ids = lax.broadcasted_iota(jnp.int32, (BLOCK_ROWS, BLOCK_ROWS), 0)
@@ -201,13 +214,17 @@
             bands[j] = (jnp.where(inside, share, 0.0) - jnp.where(back == 0, 1.0, 0.0)).astype(BF16)
         state[...] = jnp.zeros_like(state)
 
-    with jax.named_scope("x_rest"):
-        for c in range(1, chunks):
-            x_in(c).wait()
-            x_out(c).start()
+    with jax.named_scope("entry"):
+        pl.semaphore_wait(barrier, 1 + x_at + z_at)
+    each(0, x_at, lambda k: greet(row0 + k))
+    each(0, z_at, lambda k: greet(k * row_n + x_at))
+    with jax.named_scope("x_in"):
+        for i in range(2):
+            x_in(i).wait()
+            x_out(i).start()
     with jax.named_scope("w01"):
         for i in (0, 1):
-            w_in(i, OWN).wait()
+            w_wait(w_buf.at[i, OWN], i)
 
     tri = jnp.where(lower, 1.0, 0.0).astype(BF16)
     tri_twice = jnp.concatenate([tri, tri], axis=1)
@@ -259,47 +276,56 @@
     def put_pool(c):
         p_buf[BLOCK_ROWS + c * rows_x:BLOCK_ROWS + (c + 1) * rows_x, :] = proj(2, c).astype(BF16)
 
+    with jax.named_scope("own"):
+        for c in (0, 1):
+            own = x_buf[OWN, rows_of(c), :]
+            for i in (0, 1):
+                r_buf[rows_of(c), i * chans:(i + 1) * chans] = dot(own, w_buf[i, OWN])
+    with jax.named_scope("x_in2"):
+        x_in(2).wait()
+        x_out(2).start()
+
+    def rest(i, c):
+        return (r_buf[rows_of(c), i * chans:(i + 1) * chans] + dot(x_buf[PEER, rows_of(c), :], w_buf[i, PEER])).astype(BF16)
+
+    with jax.named_scope("x_recv0"):
+        x_out(0).wait_recv()
+        w_wait(w_buf.at[0:2, PEER], 2)
+        for copy in smalls[1:]:
+            copy.wait()
+    for i in (2, 3, 4):
+        for side in (OWN, PEER):
+            w_in(i, side).start()
     with jax.named_scope("first0"):
-        own = x_buf[OWN, rows_of(0), :]
-        f_own = dot(own, w_buf[0, OWN])
-        v_own = dot(own, w_buf[1, OWN])
-        with jax.named_scope("x_recv0"):
-            x_out(0).wait_recv()
-            for i in (0, 1):
-                w_in(i, PEER).wait()
-            for copy in smalls[1:]:
-                copy.wait()
-        for i in (2, 3, 4):
-            for side in (OWN, PEER):
-                w_in(i, side).start()
-        for i in range(2):
-            wo_in(i).start()
-            wo_out(i).start()
-        other = x_buf[PEER, rows_of(0), :]
-        f_buf[rows_of(0), :] = (f_own + dot(other, w_buf[0, PEER])).astype(BF16)
-        v_buf[rows_of(0), :] = (v_own + dot(other, w_buf[1, PEER])).astype(BF16)
-
+        f_buf[rows_of(0), :] = rest(0, 0)
+        v_buf[rows_of(0), :] = rest(1, 0)
+    with jax.named_scope("x_recv1"):
+        x_out(1).wait_recv()
     for c in range(1, chunks):
+        if c == 2:
+            with jax.named_scope("x_recv2"):
+                x_out(2).wait_recv()
+            for i in range(2):
+                wo_in(i).start()
+                wo_out(i).start()
+
+            @pl.when(leads)
+            def _():
+                with jax.named_scope("lead"):
+                    pl.semaphore_wait(ready, later)
+                greet(sp - 1)
+
         with jax.named_scope("first"):
-            with jax.named_scope("x_recv"):
-                x_out(c).wait_recv()
-            if c == 2:
-                @pl.when(leads)
-                def _():
-                    with jax.named_scope("lead"):
-                        pl.semaphore_wait(barrier, later)
-                    greet(sp - 1)
             post = Post(c - 1)
             post.logs()
-            f_buf[rows_of(c), :] = proj(0, c).astype(BF16)
+            f_buf[rows_of(c), :] = rest(0, c) if c == 1 else proj(0, c).astype(BF16)
             post.sums()
-            v_buf[rows_of(c), :] = proj(1, c).astype(BF16)
+            v_buf[rows_of(c), :] = rest(1, c) if c == 1 else proj(1, c).astype(BF16)
             post.exps()
             post.states()
 
     with jax.named_scope("w2"):
-        for side in (OWN, PEER):
-            w_in(2, side).wait()
+        w_wait(w_buf.at[2], 3)
     with jax.named_scope("second0"):
         post = Post(chunks - 1)
         post.logs()
@@ -319,7 +345,7 @@
     @pl.when(jnp.logical_not(leads) & (sp + 1 < n_sp))
     def _():
         with jax.named_scope("later"):
-            pl.semaphore_wait(barrier, later)
+            pl.semaphore_wait(ready, later)
 
     for step in range(1, row_n):
         mine_to(lax.rem(x_at + step, row_n), x_at).start()
@@ -334,17 +360,14 @@
             put_pool(c)
 
     with jax.named_scope("w34"):
-        for i in (3, 4):
-            for side in (OWN, PEER):
-                w_in(i, side).wait()
+        w_wait(w_buf.at[3:5], 4)
 
     def part_of(ref, at):
         return ref[at, 0:DK, :].astype(F32), ref[at, DK:DK + HALO, :].astype(F32)[0:1]
 
     def fold_row():
-        for step in range(1, row_n):
-            with jax.named_scope("row_recv"):
-                mine_to(x_at, lax.rem(x_at + step, row_n)).wait_recv()
+        with jax.named_scope("row_recv"):
+            some(row_in, row_n - 1, m_send, m_recv).wait_recv()
         total, kept = part_of(row_in, 0)
         for k in range(1, row_n):
             term, keep = part_of(row_in, k)
@@ -356,10 +379,10 @@
 
     def fold_column():
         state[:, 0:DK] = jnp.zeros((DK, DK), F32)
+        with jax.named_scope("col_recv"):
+            when_equal(z_at, range(1, col_n), lambda n: some(total_in, n, r_send, r_recv).wait_recv())
 
         def take(k):
-            with jax.named_scope("col_recv"):
-                total_to(z_at, k).wait_recv()
             term, keep = part_of(total_in, k)
             state[:, 0:DK] = keep * state[:, 0:DK] + term
 
@@ -385,7 +408,6 @@
         def __init__(self, c):
             self.c, self.rows = c, rows_of(c)
             self.blocks = [c * per + k for k in range(per)]
-            self.diff, self.scores = {}, {}
 
         def query(self):
             q_in = proj(3, self.c).astype(BF16).astype(F32)
@@ -397,40 +419,52 @@
                 for j in range(groups):
                     lanes = slice(j * GROUP_CH, (j + 1) * GROUP_CH)
                     if b:
-                        self.diff[b, j] = dot(bands[j], near[:, lanes]).astype(BF16)
+                        a_buf[OWN, block_of(b), lanes] = dot(bands[j], near[:, lanes]).astype(BF16)
                         continue
                     window = jnp.left_shift(jnp.int32(2), tp * groups + j)
                     inside = jnp.where((back >= 0) & (back < window), 1.0, 0.0).astype(BF16)
                     share = 1.0 / jnp.minimum(count, window).astype(F32)
                     share = jnp.concatenate([share] * (GROUP_CH // LANES), axis=1)
                     sums = dot(inside, near[:, lanes])
-                    self.diff[b, j] = (sums * share - near[BLOCK_ROWS:, lanes].astype(F32)).astype(BF16)
+                    a_buf[OWN, block_of(b), lanes] = (sums * share - near[BLOCK_ROWS:, lanes].astype(F32)).astype(BF16)
 
         def gates(self):
             g_buf[self.rows, :] = proj(4, self.c).astype(BF16)
 
         def mixed(self):
-            for b in self.blocks:
-                for j in range(groups):
-                    lanes = slice(j * GROUP_CH, (j + 1) * GROUP_CH)
-                    a_buf[OWN, block_of(b), lanes] = (dot(self.diff[b, j], mix[j]) * scale[:, lanes]).astype(BF16)
+            for j in range(groups):
+                lanes = slice(j * GROUP_CH, (j + 1) * GROUP_CH)
+                a_buf[OWN, self.rows, lanes] = (dot(a_buf[OWN, self.rows, lanes], mix[j]) * scale[:, lanes]).astype(BF16)
 
         def score(self):
             for b in self.blocks:
                 for h in range(heads):
                     up, down = q_buf[block_of(b), head_of(h)], u_buf[block_of(b), head_of(h)]
-                    self.scores[b, h] = jnp.where(lower, dot(up, down, NT), 0.0).astype(BF16)
+                    f_buf[block_of(b), head_of(h)] = jnp.where(lower, dot(up, down, NT), 0.0).astype(BF16)
 
         def inner(self):
             for b in self.blocks:
                 for h in range(heads):
-                    e_buf[block_of(b), head_of(h)] = dot(self.scores[b, h], v_buf[block_of(b), head_of(h)])
+                    at = block_of(b), head_of(h)
+                    e_buf[at] = dot(f_buf[at], v_buf[at])
+
+    parts = [Third(c) for c in range(chunks)]
+    early = x_at >= row_n // 2
+
+    def fold_at(stage, who):
+        @pl.when(who)
+        def _():
+            stage()
 
     for c in reversed(range(chunks)):
-        if c == 1:
-            fold_row()
+        if c == chunks - 2:
+            fold_at(fold_row, early)
+        if c == chunks - 3:
+            pool_out(0).start()
+            fold_at(fold_column, early)
+            fold_at(fold_row, jnp.logical_not(early))
         if c == 0:
-            fold_column()
+            fold_at(fold_column, jnp.logical_not(early))
 
             @pl.when(sp > 0)
             def _():
@@ -439,19 +473,19 @@
                 p_buf[BLOCK_ROWS - HALO:BLOCK_ROWS, :] = halo_in[...]
 
         with jax.named_scope("third"):
-            part = Third(c)
-            part.query()
-            part.band()
-            part.gates()
-            part.mixed()
-            part.score()
-            part.inner()
-            a_out(0, c).start()
+            parts[c].query()
+            if c + 1 < chunks:
+                parts[c + 1].inner()
+            parts[c].band()
+            parts[c].gates()
+            parts[c].mixed()
+            parts[c].score()
+    pool_out(1).start()
 
     with jax.named_scope("wo"):
-        for i in range(2):
-            wo_in(i).wait()
-            wo_out(i).wait_recv()
+        pltpu.make_async_copy(wo_buf.at[OWN], wo_buf.at[OWN], wo_loc).wait()
+        to_peer(wo_buf.at[OWN], wo_buf.at[PEER], wo_send, wo_recv).wait_recv()
+        pool_out(0).wait_recv()
 
     pool_at, rec_at = slice(0, pool_w), slice(pool_w, pool_w + chans)
 
@@ -462,18 +496,14 @@
             + ALPHA * x_buf[OWN, rows, :].astype(F32))
 
     with jax.named_scope("pool"):
-        for c in reversed(range(2, chunks)):
-            a_out(0, c).wait_recv()
-        for c in reversed(range(2, chunks)):
-            pool_part(c)
-
-    for step in range(1, row_n):
-        k = lax.rem(x_at + step, row_n)
-
-        @pl.when(sp > 0)
-        def _():
-            with jax.named_scope("start_recv"):
-                start_to(x_at, k).wait_recv()
+        pool_part(chunks - 1)
+        parts[0].inner()
+        pool_part(chunks - 2)
+
+    @pl.when(sp > 0)
+    def _():
+        with jax.named_scope("start_recv"):
+            some(start_in, row_n - 1, b_send, b_recv).wait_recv()
 
     @pl.when(sp > 0)
     def _():
@@ -499,13 +529,24 @@
                 rec = raw * lax.rsqrt(power + EPS_RMS) * gain[...] * (gate * half_sigmoid(gate))
                 a_buf[OWN, block_of(b), pool_w + h * DK:pool_w + (h + 1) * DK] = rec.astype(BF16)
 
-    for c in range(chunks):
-        with jax.named_scope("fourth"):
-            fourth(c)
-            if c < 2:
-                a_out(0, 1 - c).wait_recv()
-                pool_part(1 - c)
-            a_out(1, c).start()
+    def rec_part(side, c):
+        r_buf[rows_of(c), :] += dot(a_buf[side, rows_of(c), rec_at], wo_buf[side, rec_at])
+
+    with jax.named_scope("fourth"):
+        fourth(0)
+        with jax.named_scope("pool_recv"):
+            pool_out(1).wait_recv()
+        pool_part(1)
+        fourth(1)
+        pool_part(0)
+        rec_out(0).start()
+    with jax.named_scope("fourth2"):
+        fourth(2)
+        rec_part(OWN, 0)
+        rec_out(1).start()
+        fourth(3)
+        rec_part(OWN, 1)
+        rec_out(2).start()
 
     def fold(x):
         acc = x[:, :LANES]
@@ -515,44 +556,47 @@
 
     first_half = lax.broadcasted_iota(jnp.int32, (rows_x, LANES), 1) < LANES // 2
 
-    for c in range(chunks):
-        with jax.named_scope("fifth"):
-            rows = rows_of(c)
-            a_out(1, c).wait_recv()
-            resid = r_buf[rows, :] + (
-                dot(a_buf[OWN, rows, rec_at], wo_buf[OWN, rec_at]) + dot(a_buf[PEER, rows, rec_at], wo_buf[PEER, rec_at]))
-            r_buf[rows, :] = resid
-            sums, squares = fold(resid), fold(resid * resid)
-            sums = sums + pltpu.roll(sums, LANES // 2, 1)
-            squares = squares + pltpu.roll(squares, LANES // 2, 1)
-            stat_own[c] = jnp.where(first_half, sums, squares)
-            s_out(c).start()
-
-    with jax.named_scope("tail"):
-        for c in range(chunks):
-            s_out(c).wait_recv()
-            stats[rows_of(c), :] = stat_own[c] + stat_peer[c]
-
-        for c in range(chunks):
-            x_out(c).wait_send()
-            s_out(c).wait_send()
-            for i in range(2):
-                a_out(i, c).wait_send()
-        for i in range(2):
-            wo_out(i).wait_send()
-        for step in range(1, row_n):
-            k = lax.rem(x_at + step, row_n)
-            mine_to(k, x_at).wait_send()
-
-            @pl.when(row0 + k > 0)
-            def _():
-                start_to(k, x_at).wait_send()
-
-        each(z_at + 1, col_n, lambda k: total_to(k, z_at).wait_send())
+    def fifth(c):
+        rows = rows_of(c)
+        resid = r_buf[rows, :] + dot(a_buf[PEER, rows, rec_at], wo_buf[PEER, rec_at])
+        r_buf[rows, :] = resid
+        sums, squares = fold(resid), fold(resid * resid)
+        sums = sums + pltpu.roll(sums, LANES // 2, 1)
+        squares = squares + pltpu.roll(squares, LANES // 2, 1)
+        stat_own[rows, :] = jnp.where(first_half, sums, squares)
+
+    with jax.named_scope("fifth"):
+        rec_out(0).wait_recv()
+        fifth(0)
+        fifth(1)
+        rec_part(OWN, 2)
+        s_out(0).start()
+    with jax.named_scope("fifth2"):
+        rec_out(1).wait_recv()
+        fifth(2)
+        rec_part(OWN, 3)
+        rec_out(2).wait_recv()
+        fifth(3)
+        s_out(1).start()
+
+    with jax.named_scope("sent"):
+        to_peer(x_buf.at[OWN], x_buf.at[PEER], x_send, x_recv.at[0]).wait_send()
+        to_peer(a_buf.at[OWN], a_buf.at[PEER], a_send, a_recv.at[0]).wait_send()
+        to_peer(wo_buf.at[OWN], wo_buf.at[PEER], wo_send, wo_recv).wait_send()
+        some(mine_out, row_n - 1, m_send, m_recv).wait_send()
+        when_equal(col_n - 1 - z_at, range(1, col_n), lambda n: some(total_in, n, r_send, r_recv).wait_send())
+        starts = jnp.where((z_at > 0) | (x_at == 0), row_n - 1, row_n - 2)
+        when_equal(starts, (row_n - 2, row_n - 1), lambda n: some(start_out, n, b_send, b_recv).wait_send())
 
         @pl.when(sp + 1 < n_sp)
         def _():
             h_out(sp + 1).wait_send()
+
+    with jax.named_scope("tail"):
+        for i in range(2):
+            s_out(i).wait_recv()
+        stats[...] = stat_own[...] + stat_peer[...]
+        to_peer(stat_own, stat_peer, s_send, s_recv.at[0]).wait_send()
 
 
 def finish(width, rows, resid, stats, gain, bias, out, o_buf, o_sem):
@@ -611,18 +655,16 @@
             pltpu.VMEM((heads, DK, DK), BF16),
             pltpu.VMEM((heads, DK, DK), BF16),
             pltpu.VMEM((HALO, pool_w), BF16),
-            pltpu.VMEM((chunks, rows_x, LANES), F32),
-            pltpu.VMEM((chunks, rows_x, LANES), F32),
+            pltpu.VMEM((length, LANES), F32),
+            pltpu.VMEM((length, LANES), F32),
             pltpu.VMEM((mix.shape[0], BLOCK_ROWS, 2 * BLOCK_ROWS), BF16),
             pltpu.VMEM(mix.shape, BF16),
             pltpu.VMEM((1, pool_w), F32),
             pltpu.VMEM((1, chans), F32),
             pltpu.VMEM((heads, length), F32),
             pltpu.VMEM((1, DK), F32),
-            dma((chunks,)), dma((chunks,)), dma((chunks,)), dma((5, n_tp)),
-            dma((2,)), dma((2,)), dma((2,)), dma((2, chunks)), dma((2, chunks)),
-            dma((heads,)), dma((heads,)), dma((n_sp // heads,)), dma((n_sp // heads,)),
-            dma((heads,)), dma((heads,)), dma, dma, dma((chunks,)), dma((chunks,)), dma((5,)),
+            dma((3,)), dma, dma((3,)), dma((5,)), dma, dma, dma, dma, dma((5,)),
+            dma, dma, dma, dma, dma, dma, dma, dma, dma, dma((2,)), dma((5,)), pltpu.SemaphoreType.REGULAR,
         ]
         row = lambda x: x.reshape(1, -1)
         resid, stats = pl.pallas_call(

time: 34.6 us -> 31.8 us (0.919)
  Pallas kernels: 34.3 us -> 31.5 us
    pallas_call x1, Pallas kernels: 32.4 us -> 29.6 us  [local(): pl.pallas_call(functools.partial(mixer, n_sp, n_tp, rows_x), out_shape=(p...]
where the time goes in v3:
time: 31.8 us; the launch traced here: 31.7 us
  Pallas kernels  31.5 us (99%)
    pallas_call x1, Pallas kernels, local(): pl.pallas_call(functools.partial(mixer, n_sp, n_tp, rows_x), out_shape=(p...  29.6 us
    pallas_call x1, Pallas kernels, local(): pl.pallas_call(functools.partial(finish, n_tp * feats, piece), out_shape=...  1.85 us

profile of v3, /device:TPU:81, one launch (start us, length us, event | category | flops | bytes accessed | tf_op | source)
XLA Modules:
  0.0 31.7 jit_solution(2723227879117607571)
XLA Ops:
  0.0 0.0 copy-start
  0.0 0.0 copy-start.1
  0.0 29.6 %mixer.1 = (f32[1024,1024]{1,0:T(8,128)S(1)}, f32[1024,128]{1,0:T(8,128)S(1)}) custom-call(bf16[1,1024,1024]{2,1,0:T(8,128)(2,1)} %stream.1, bf16[2048,512]{1,0:T(8,128)(2,1)} %w_pool.1, bf16[2048,512]{1,0:T(8,128)(2,1)} %w_query.1, bf16[2048,512]{1,0:T(8,128)(2,1)} %w_forget.1, bf16[2048,512]{1,0:T(8,128)(2,1)} %w_value.1, bf16[2048,512]{1,0:T(8,128)(2,1)} %w_gate.1, ...), custom_call_target="tpu_custom_call" | custom-call | tf_op jit(solution)/shard_map/mixer/pallas_call | solution.py:670
  29.6 0.0 copy-done
  29.6 0.0 copy-done.1
  29.6 1.8 %finish.1 = bf16[1,1024,1024]{2,1,0:T(8,128)(2,1)} custom-call(f32[1024,1024]{1,0:T(8,128)S(1)} %get-tuple-element.7.resid, f32[1024,128]{1,0:T(8,128)S(1)} %get-tuple-element.8.stats, f32[1,1024]{1,0:T(1,128)S(1)} %bitcast.6, f32[1,1024]{1,0:T(1,128)S(1)} %bitcast.7), custom_call_target="tpu_custom_call" | custom-call | tf_op jit(solution)/shard_map/finish/pallas_call | solution.py:683
Async XLA Ops:
  0.0 29.6 %copy-start = (f32[1024]{0:T(1024)S(1)}, f32[1024]{0:T(1024)}, u32[]{:S(2)}) copy-start(f32[1024]{0:T(1024)} %param.28) | copy-start | bytes 12292
  0.0 29.6 %copy-start.1 = (f32[1024]{0:T(1024)S(1)}, f32[1024]{0:T(1024)}, u32[]{:S(2)}) copy-start(f32[1024]{0:T(1024)} %param.29) | copy-start | bytes 12292

commit v4 on v3

--- a/solution.py
+++ b/solution.py
@@ -71,10 +71,10 @@
     def head_of(h):
         return slice(h * DK, (h + 1) * DK)
 
-    x_pieces = ((0, rows_x), (rows_x, rows_x), (2 * rows_x, length - 2 * rows_x))
-    pool_pieces = ((length // 2, length // 2), (0, length // 2))
+    x_pieces = ((0, length // 2), (length // 2, length // 2))
+    pool_pieces = ((2 * rows_x, length - 2 * rows_x), (rows_x, rows_x), (0, rows_x))
     rec_pieces = ((0, 2 * rows_x),) + tuple((c * rows_x, rows_x) for c in range(2, chunks))
-    stat_pieces = ((0, length // 2), (length // 2, length // 2))
+    stat_pieces = rec_pieces
 
     def to_peer(src, dst, send, recv):
         return pltpu.make_async_remote_copy(
@@ -163,16 +163,10 @@
             ((extra_in, extra), (bound_in, bound), (mix_in, mix), (scale_in, scale), (gain_in, gain)))
     ]
 
+    x_in(0).start()
     smalls[0].start()
-    x_in(0).start()
     x_in(1).start()
     w_in(0, OWN).start()
-    w_in(1, OWN).start()
-    x_in(2).start()
-    w_in(0, PEER).start()
-    w_in(1, PEER).start()
-    for copy in smalls[1:]:
-        copy.start()
 
     barrier = pltpu.get_barrier_semaphore()
     pl.semaphore_signal(barrier, inc=1, device_id={"tp": peer}, device_id_type=mesh_id)
@@ -188,6 +182,11 @@
     p_buf[0:BLOCK_ROWS, :] = jnp.zeros((BLOCK_ROWS, pool_w), BF16)
     with jax.named_scope("extra"):
         smalls[0].wait()
+    w_in(1, OWN).start()
+    w_in(0, PEER).start()
+    w_in(1, PEER).start()
+    for copy in smalls[1:]:
+        copy.start()
 
     row_ids = lax.broadcasted_iota(jnp.int32, (BLOCK_ROWS, BLOCK_ROWS), 0)
     col_ids = lax.broadcasted_iota(jnp.int32, (BLOCK_ROWS, BLOCK_ROWS), 1)
@@ -222,15 +221,14 @@
         for i in range(2):
             x_in(i).wait()
             x_out(i).start()
-    with jax.named_scope("w01"):
-        for i in (0, 1):
-            w_wait(w_buf.at[i, OWN], i)
+    with jax.named_scope("w0"):
+        w_wait(w_buf.at[0, OWN], 0)
 
     tri = jnp.where(lower, 1.0, 0.0).astype(BF16)
     tri_twice = jnp.concatenate([tri, tri], axis=1)
 
-    def proj(i, c):
-        rows = rows_of(c)
+    def proj(i, c, part=slice(0, rows_x)):
+        rows = slice(c * rows_x + part.start, c * rows_x + part.stop)
         return dot(x_buf[OWN, rows, :], w_buf[i, OWN]) + dot(x_buf[PEER, rows, :], w_buf[i, PEER])
 
     class Post:
@@ -273,17 +271,22 @@
                     t_buf[b, :, lanes] = term
                     state[:, lanes] = hh * hh * state[:, lanes] + term
 
-    def put_pool(c):
-        p_buf[BLOCK_ROWS + c * rows_x:BLOCK_ROWS + (c + 1) * rows_x, :] = proj(2, c).astype(BF16)
-
-    with jax.named_scope("own"):
-        for c in (0, 1):
-            own = x_buf[OWN, rows_of(c), :]
-            for i in (0, 1):
-                r_buf[rows_of(c), i * chans:(i + 1) * chans] = dot(own, w_buf[i, OWN])
-    with jax.named_scope("x_in2"):
-        x_in(2).wait()
-        x_out(2).start()
+    whole, upper, under = slice(0, rows_x), slice(0, rows_x // 2), slice(rows_x // 2, rows_x)
+
+    def put_pool(c, part=whole):
+        at = BLOCK_ROWS + c * rows_x
+        p_buf[at + part.start:at + part.stop, :] = proj(2, c, part).astype(BF16)
+
+    def own_half(i):
+        for c in range(chunks):
+            r_buf[rows_of(c), i * chans:(i + 1) * chans] = dot(x_buf[OWN, rows_of(c), :], w_buf[i, OWN])
+
+    with jax.named_scope("own0"):
+        own_half(0)
+    with jax.named_scope("w1"):
+        w_wait(w_buf.at[1, OWN], 1)
+    with jax.named_scope("own1"):
+        own_half(1)
 
     def rest(i, c):
         return (r_buf[rows_of(c), i * chans:(i + 1) * chans] + dot(x_buf[PEER, rows_of(c), :], w_buf[i, PEER])).astype(BF16)
@@ -296,15 +299,10 @@
     for i in (2, 3, 4):
         for side in (OWN, PEER):
             w_in(i, side).start()
-    with jax.named_scope("first0"):
-        f_buf[rows_of(0), :] = rest(0, 0)
-        v_buf[rows_of(0), :] = rest(1, 0)
-    with jax.named_scope("x_recv1"):
-        x_out(1).wait_recv()
-    for c in range(1, chunks):
+    for c in range(chunks):
         if c == 2:
-            with jax.named_scope("x_recv2"):
-                x_out(2).wait_recv()
+            with jax.named_scope("x_recv1"):
+                x_out(1).wait_recv()
             for i in range(2):
                 wo_in(i).start()
                 wo_out(i).start()
@@ -316,13 +314,16 @@
                 greet(sp - 1)
 
         with jax.named_scope("first"):
-            post = Post(c - 1)
-            post.logs()
-            f_buf[rows_of(c), :] = rest(0, c) if c == 1 else proj(0, c).astype(BF16)
-            post.sums()
-            v_buf[rows_of(c), :] = rest(1, c) if c == 1 else proj(1, c).astype(BF16)
-            post.exps()
-            post.states()
+            if c:
+                post = Post(c - 1)
+                post.logs()
+            f_buf[rows_of(c), :] = rest(0, c)
+            if c:
+                post.sums()
+            v_buf[rows_of(c), :] = rest(1, c)
+            if c:
+                post.exps()
+                post.states()
 
     with jax.named_scope("w2"):
         w_wait(w_buf.at[2], 3)
@@ -355,12 +356,11 @@
     def _():
         h_out(sp + 1).start()
 
+    with jax.named_scope("w34"):
+        w_wait(w_buf.at[3:5], 4)
     with jax.named_scope("second"):
         for c in range(chunks - 2):
             put_pool(c)
-
-    with jax.named_scope("w34"):
-        w_wait(w_buf.at[3:5], 4)
 
     def part_of(ref, at):
         return ref[at, 0:DK, :].astype(F32), ref[at, DK:DK + HALO, :].astype(F32)[0:1]
@@ -403,6 +403,8 @@
         start_in[x_at] = start_out[x_at]
 
     count = lax.broadcasted_iota(jnp.int32, (BLOCK_ROWS, LANES), 0) + (sp * length + 1)
+
+    gains = jnp.concatenate([gain[...]] * heads, axis=1)
 
     class Third:
         def __init__(self, c):
@@ -428,8 +430,10 @@
                     sums = dot(inside, near[:, lanes])
                     a_buf[OWN, block_of(b), lanes] = (sums * share - near[BLOCK_ROWS:, lanes].astype(F32)).astype(BF16)
 
-        def gates(self):
-            g_buf[self.rows, :] = proj(4, self.c).astype(BF16)
+        def gates(self, part):
+            rows = slice(self.rows.start + part.start, self.rows.start + part.stop)
+            gate = proj(4, self.c, part).astype(BF16).astype(F32)
+            g_buf[rows, :] = gate * half_sigmoid(gate) * gains
 
         def mixed(self):
             for j in range(groups):
@@ -449,7 +453,7 @@
                     e_buf[at] = dot(f_buf[at], v_buf[at])
 
     parts = [Third(c) for c in range(chunks)]
-    early = x_at >= row_n // 2
+    early = x_at > 0
 
     def fold_at(stage, who):
         @pl.when(who)
@@ -457,14 +461,13 @@
             stage()
 
     for c in reversed(range(chunks)):
-        if c == chunks - 2:
+        if c == 1:
+            pool_out(0).start()
             fold_at(fold_row, early)
-        if c == chunks - 3:
-            pool_out(0).start()
+        if c == 0:
+            pool_out(1).start()
             fold_at(fold_column, early)
             fold_at(fold_row, jnp.logical_not(early))
-        if c == 0:
-            fold_at(fold_column, jnp.logical_not(early))
 
             @pl.when(sp > 0)
             def _():
@@ -477,10 +480,11 @@
             if c + 1 < chunks:
                 parts[c + 1].inner()
             parts[c].band()
-            parts[c].gates()
+            parts[c].gates(whole)
             parts[c].mixed()
             parts[c].score()
-    pool_out(1).start()
+    pool_out(2).start()
+    fold_at(fold_column, jnp.logical_not(early))
 
     with jax.named_scope("wo"):
         pltpu.make_async_copy(wo_buf.at[OWN], wo_buf.at[OWN], wo_loc).wait()
@@ -499,6 +503,13 @@
         pool_part(chunks - 1)
         parts[0].inner()
         pool_part(chunks - 2)
+    with jax.named_scope("pool_recv"):
+        pool_out(1).wait_recv()
+    with jax.named_scope("pool"):
+        pool_part(1)
+
+    with jax.named_scope("pool_recv"):
+        pool_out(2).wait_recv()
 
     @pl.when(sp > 0)
     def _():
@@ -525,8 +536,7 @@
                 lanes = head_of(h)
                 raw = e_buf[block_of(b), lanes] + dot(q_buf[block_of(b), lanes], carried[:, lanes], NT)
                 power = jnp.mean(raw * raw, axis=-1, keepdims=True)
-                gate = g_buf[block_of(b), lanes].astype(F32)
-                rec = raw * lax.rsqrt(power + EPS_RMS) * gain[...] * (gate * half_sigmoid(gate))
+                rec = raw * lax.rsqrt(power + EPS_RMS) * g_buf[block_of(b), lanes]
                 a_buf[OWN, block_of(b), pool_w + h * DK:pool_w + (h + 1) * DK] = rec.astype(BF16)
 
     def rec_part(side, c):
@@ -534,11 +544,8 @@
 
     with jax.named_scope("fourth"):
         fourth(0)
-        with jax.named_scope("pool_recv"):
-            pool_out(1).wait_recv()
-        pool_part(1)
+        pool_part(0)
         fourth(1)
-        pool_part(0)
         rec_out(0).start()
     with jax.named_scope("fourth2"):
         fourth(2)
@@ -575,9 +582,11 @@
         rec_out(1).wait_recv()
         fifth(2)
         rec_part(OWN, 3)
+        s_out(1).start()
+    with jax.named_scope("fifth3"):
         rec_out(2).wait_recv()
         fifth(3)
-        s_out(1).start()
+        s_out(2).start()
 
     with jax.named_scope("sent"):
         to_peer(x_buf.at[OWN], x_buf.at[PEER], x_send, x_recv.at[0]).wait_send()
@@ -593,7 +602,7 @@
             h_out(sp + 1).wait_send()
 
     with jax.named_scope("tail"):
-        for i in range(2):
+        for i in range(len(stat_pieces)):
             s_out(i).wait_recv()
         stats[...] = stat_own[...] + stat_peer[...]
         to_peer(stat_own, stat_peer, s_send, s_recv.at[0]).wait_send()
@@ -644,7 +653,7 @@
             pltpu.VMEM((blocks, DK, chans), F32),
             pltpu.VMEM((BLOCK_ROWS + length, pool_w), BF16),
             pltpu.VMEM((length, chans), BF16),
-            pltpu.VMEM((length, chans), BF16),
+            pltpu.VMEM((length, chans), F32),
             pltpu.VMEM((length, chans), BF16),
             pltpu.VMEM((blocks, 8, chans), F32),
             pltpu.VMEM((DK, chans), F32),
@@ -663,8 +672,8 @@
             pltpu.VMEM((1, chans), F32),
             pltpu.VMEM((heads, length), F32),
             pltpu.VMEM((1, DK), F32),
-            dma((3,)), dma, dma((3,)), dma((5,)), dma, dma, dma, dma, dma((5,)),
-            dma, dma, dma, dma, dma, dma, dma, dma, dma, dma((2,)), dma((5,)), pltpu.SemaphoreType.REGULAR,
+            dma((2,)), dma, dma((2,)), dma((5,)), dma, dma, dma, dma, dma((6,)),
+            dma, dma, dma, dma, dma, dma, dma, dma, dma, dma((3,)), dma((5,)), pltpu.SemaphoreType.REGULAR,
         ]
         row = lambda x: x.reshape(1, -1)
         resid, stats = pl.pallas_call(

time: 31.8 us -> 30.6 us (0.962)
  Pallas kernels: 31.5 us -> 30.3 us
    pallas_call x1, Pallas kernels: 29.6 us -> 28.4 us  [local(): pl.pallas_call(functools.partial(mixer, n_sp, n_tp, rows_x), out_shape=(p...]
where the time goes in v4:
time: 30.6 us; the launch traced here: 30.5 us
  Pallas kernels  30.3 us (99%)
    pallas_call x1, Pallas kernels, local(): pl.pallas_call(functools.partial(mixer, n_sp, n_tp, rows_x), out_shape=(p...  28.4 us
    pallas_call x1, Pallas kernels, local(): pl.pallas_call(functools.partial(finish, n_tp * feats, piece), out_shape=...  1.85 us

profile of v4, /device:TPU:81, one launch (start us, length us, event | category | flops | bytes accessed | tf_op | source)
XLA Modules:
  0.0 30.5 jit_solution(4367476640738252321)
XLA Ops:
  0.0 0.0 copy-start
  0.0 0.0 copy-start.1
  0.0 28.4 %mixer.1 = (f32[1024,1024]{1,0:T(8,128)S(1)}, f32[1024,128]{1,0:T(8,128)S(1)}) custom-call(bf16[1,1024,1024]{2,1,0:T(8,128)(2,1)} %stream.1, bf16[2048,512]{1,0:T(8,128)(2,1)} %w_pool.1, bf16[2048,512]{1,0:T(8,128)(2,1)} %w_query.1, bf16[2048,512]{1,0:T(8,128)(2,1)} %w_forget.1, bf16[2048,512]{1,0:T(8,128)(2,1)} %w_value.1, bf16[2048,512]{1,0:T(8,128)(2,1)} %w_gate.1, ...), custom_call_target="tpu_custom_call" | custom-call | tf_op jit(solution)/shard_map/mixer/pallas_call | solution.py:679
  28.5 0.0 copy-done
  28.5 0.0 copy-done.1
  28.5 1.8 %finish.1 = bf16[1,1024,1024]{2,1,0:T(8,128)(2,1)} custom-call(f32[1024,1024]{1,0:T(8,128)S(1)} %get-tuple-element.7.resid, f32[1024,128]{1,0:T(8,128)S(1)} %get-tuple-element.8.stats, f32[1,1024]{1,0:T(1,128)S(1)} %bitcast.6, f32[1,1024]{1,0:T(1,128)S(1)} %bitcast.7), custom_call_target="tpu_custom_call" | custom-call | tf_op jit(solution)/shard_map/finish/pallas_call | solution.py:692
Async XLA Ops:
  0.0 28.5 %copy-start = (f32[1024]{0:T(1024)S(1)}, f32[1024]{0:T(1024)}, u32[]{:S(2)}) copy-start(f32[1024]{0:T(1024)} %param.28) | copy-start | bytes 12292
  0.0 28.5 %copy-start.1 = (f32[1024]{0:T(1024)S(1)}, f32[1024]{0:T(1024)}, u32[]{:S(2)}) copy-start(f32[1024]{0:T(1024)} %param.29) | copy-start | bytes 12292

commit v5 on v4

--- a/solution.py
+++ b/solution.py
@@ -73,8 +73,8 @@
 
     x_pieces = ((0, length // 2), (length // 2, length // 2))
     pool_pieces = ((2 * rows_x, length - 2 * rows_x), (rows_x, rows_x), (0, rows_x))
-    rec_pieces = ((0, 2 * rows_x),) + tuple((c * rows_x, rows_x) for c in range(2, chunks))
-    stat_pieces = rec_pieces
+    rec_pieces = tuple((c * rows_x, rows_x) for c in range(chunks))
+    stat_pieces = ((0, length - rows_x), (length - rows_x, rows_x))
 
     def to_peer(src, dst, send, recv):
         return pltpu.make_async_remote_copy(
@@ -163,10 +163,10 @@
             ((extra_in, extra), (bound_in, bound), (mix_in, mix), (scale_in, scale), (gain_in, gain)))
     ]
 
+    smalls[0].start()
     x_in(0).start()
-    smalls[0].start()
+    w_in(0, OWN).start()
     x_in(1).start()
-    w_in(0, OWN).start()
 
     barrier = pltpu.get_barrier_semaphore()
     pl.semaphore_signal(barrier, inc=1, device_id={"tp": peer}, device_id_type=mesh_id)
@@ -180,47 +180,37 @@
     ends = (x_at == row_n - 1) & (z_at < col_n - 1)
     later = (row_n - 1 - x_at) + (col_n - 1 - z_at) + jnp.where(ends, 1, 0)
     p_buf[0:BLOCK_ROWS, :] = jnp.zeros((BLOCK_ROWS, pool_w), BF16)
-    with jax.named_scope("extra"):
-        smalls[0].wait()
+
+    row_ids = lax.broadcasted_iota(jnp.int32, (BLOCK_ROWS, BLOCK_ROWS), 0)
+    col_ids = lax.broadcasted_iota(jnp.int32, (BLOCK_ROWS, BLOCK_ROWS), 1)
+    lower = row_ids >= col_ids
+
+    state[...] = jnp.zeros_like(state)
+    with jax.named_scope("entry"):
+        pl.semaphore_wait(barrier, 1 + x_at + z_at)
+    with jax.named_scope("x_in"):
+        x_in(0).wait()
+        x_out(0).start()
     w_in(1, OWN).start()
     w_in(0, PEER).start()
     w_in(1, PEER).start()
     for copy in smalls[1:]:
         copy.start()
-
-    row_ids = lax.broadcasted_iota(jnp.int32, (BLOCK_ROWS, BLOCK_ROWS), 0)
-    col_ids = lax.broadcasted_iota(jnp.int32, (BLOCK_ROWS, BLOCK_ROWS), 1)
-    lower = row_ids >= col_ids
-
-    with jax.named_scope("drops"):
-        lower_twice = jnp.concatenate([row_ids, row_ids], axis=1) >= jnp.concatenate([col_ids, col_ids], axis=1)
-        ones = jnp.ones((2 * BLOCK_ROWS, DK), BF16)
-        for b in range(blocks):
-            drop = extra[:, block_of(b)]
-            drop_high = drop.astype(BF16).astype(F32)
-            drop_low = drop - drop_high
-            for h in range(heads):
-                pair = jnp.concatenate([drop_high[h:h + 1], drop_low[h:h + 1]], axis=1)
-                wide = jnp.where(lower_twice, jnp.broadcast_to(pair, (BLOCK_ROWS, 2 * BLOCK_ROWS)), 0.0)
-                e_buf[block_of(b), head_of(h)] = dot(wide.astype(BF16), ones)
-        wide_rows = lax.broadcasted_iota(jnp.int32, (BLOCK_ROWS, 2 * BLOCK_ROWS), 0) + BLOCK_ROWS
-        wide_cols = lax.broadcasted_iota(jnp.int32, (BLOCK_ROWS, 2 * BLOCK_ROWS), 1)
-        back = wide_rows - wide_cols
+    each(0, x_at, lambda k: greet(row0 + k))
+    each(0, z_at, lambda k: greet(k * row_n + x_at))
+    wide_rows = lax.broadcasted_iota(jnp.int32, (BLOCK_ROWS, 2 * BLOCK_ROWS), 0) + BLOCK_ROWS
+    wide_cols = lax.broadcasted_iota(jnp.int32, (BLOCK_ROWS, 2 * BLOCK_ROWS), 1)
+    back = wide_rows - wide_cols
+    with jax.named_scope("bands"):
         for j in range(groups):
             window = jnp.left_shift(jnp.int32(2), tp * groups + j)
             share = 1.0 / window.astype(F32)
             inside = (back >= 0) & (back < window)
             bands[j] = (jnp.where(inside, share, 0.0) - jnp.where(back == 0, 1.0, 0.0)).astype(BF16)
-        state[...] = jnp.zeros_like(state)
-
-    with jax.named_scope("entry"):
-        pl.semaphore_wait(barrier, 1 + x_at + z_at)
-    each(0, x_at, lambda k: greet(row0 + k))
-    each(0, z_at, lambda k: greet(k * row_n + x_at))
-    with jax.named_scope("x_in"):
-        for i in range(2):
-            x_in(i).wait()
-            x_out(i).start()
+
+    with jax.named_scope("x_in1"):
+        x_in(1).wait()
+        x_out(1).start()
     with jax.named_scope("w0"):
         w_wait(w_buf.at[0, OWN], 0)
 
@@ -242,14 +232,17 @@
             for b in self.blocks:
                 f_in = f_buf[block_of(b), :].astype(F32)
                 weight = open_part * (0.5 - 0.5 * jnp.tanh(0.5 * f_in))
-                keep = jnp.log(1.0 - weight)
+                drop = jnp.concatenate([extra[:, block_of(b)], jnp.zeros((8 - heads, BLOCK_ROWS), F32)], axis=0).T
+                drop = jnp.concatenate(
+                    [jnp.broadcast_to(drop[:, h:h + 1], (BLOCK_ROWS, DK)) for h in range(heads)], axis=1)
+                keep = jnp.log(1.0 - weight) + drop
                 high = keep.astype(BF16)
                 low = (keep - high.astype(F32)).astype(BF16)
                 self.weight[b], self.split[b] = weight, jnp.concatenate([high, low], axis=0)
 
         def sums(self):
             for b in self.blocks:
-                self.total[b] = dot(tri_twice, self.split[b]) + e_buf[block_of(b), :]
+                self.total[b] = dot(tri_twice, self.split[b])
 
         def exps(self):
             for b in self.blocks:
@@ -277,16 +270,18 @@
         at = BLOCK_ROWS + c * rows_x
         p_buf[at + part.start:at + part.stop, :] = proj(2, c, part).astype(BF16)
 
-    def own_half(i):
-        for c in range(chunks):
+    def own_half(i, some_chunks):
+        for c in some_chunks:
             r_buf[rows_of(c), i * chans:(i + 1) * chans] = dot(x_buf[OWN, rows_of(c), :], w_buf[i, OWN])
 
     with jax.named_scope("own0"):
-        own_half(0)
+        own_half(0, range(chunks))
     with jax.named_scope("w1"):
         w_wait(w_buf.at[1, OWN], 1)
+    for side in (OWN, PEER):
+        w_in(2, side).start()
     with jax.named_scope("own1"):
-        own_half(1)
+        own_half(1, range(chunks))
 
     def rest(i, c):
         return (r_buf[rows_of(c), i * chans:(i + 1) * chans] + dot(x_buf[PEER, rows_of(c), :], w_buf[i, PEER])).astype(BF16)
@@ -294,47 +289,59 @@
     with jax.named_scope("x_recv0"):
         x_out(0).wait_recv()
         w_wait(w_buf.at[0:2, PEER], 2)
-        for copy in smalls[1:]:
+        for copy in smalls:
             copy.wait()
-    for i in (2, 3, 4):
+    for i in (3, 4):
         for side in (OWN, PEER):
             w_in(i, side).start()
-    for c in range(chunks):
-        if c == 2:
-            with jax.named_scope("x_recv1"):
-                x_out(1).wait_recv()
-            for i in range(2):
-                wo_in(i).start()
-                wo_out(i).start()
-
-            @pl.when(leads)
-            def _():
-                with jax.named_scope("lead"):
-                    pl.semaphore_wait(ready, later)
-                greet(sp - 1)
-
-        with jax.named_scope("first"):
-            if c:
-                post = Post(c - 1)
-                post.logs()
-            f_buf[rows_of(c), :] = rest(0, c)
-            if c:
-                post.sums()
-            v_buf[rows_of(c), :] = rest(1, c)
-            if c:
-                post.exps()
-                post.states()
-
-    with jax.named_scope("w2"):
+    posts = [Post(c) for c in range(chunks)]
+
+    def forget(c):
+        f_buf[rows_of(c), :] = rest(0, c)
+
+    def value(c):
+        v_buf[rows_of(c), :] = rest(1, c)
+
+    with jax.named_scope("first"):
+        forget(0)
+        posts[0].logs()
+        forget(1)
+        posts[0].sums()
+        value(0)
+        posts[0].exps()
+    with jax.named_scope("x_recv1"):
+        x_out(1).wait_recv()
         w_wait(w_buf.at[2], 3)
-    with jax.named_scope("second0"):
-        post = Post(chunks - 1)
-        post.logs()
-        put_pool(chunks - 1)
-        post.sums()
-        put_pool(chunks - 2)
-        post.exps()
-        post.states()
+    for i in range(2):
+        wo_in(i).start()
+        wo_out(i).start()
+
+    @pl.when(leads)
+    def _():
+        with jax.named_scope("lead"):
+            pl.semaphore_wait(ready, later)
+        greet(sp - 1)
+
+    with jax.named_scope("first2"):
+        posts[1].logs()
+        forget(2)
+        posts[0].states()
+        posts[1].sums()
+        value(1)
+        posts[1].exps()
+        posts[2].logs()
+        forget(3)
+        posts[1].states()
+        posts[2].sums()
+        value(2)
+        posts[2].exps()
+        posts[3].logs()
+        posts[2].states()
+        posts[3].sums()
+        value(3)
+        posts[3].exps()
+        put_pool(3, under)
+        posts[3].states()
         log_half = half_buf[0, 0:1]
         for b in range(1, blocks):
             log_half = log_half * half_buf[b, 0:1]
@@ -359,7 +366,8 @@
     with jax.named_scope("w34"):
         w_wait(w_buf.at[3:5], 4)
     with jax.named_scope("second"):
-        for c in range(chunks - 2):
+        put_pool(3, upper)
+        for c in reversed(range(chunks - 1)):
             put_pool(c)
 
     def part_of(ref, at):
@@ -453,7 +461,7 @@
                     e_buf[at] = dot(f_buf[at], v_buf[at])
 
     parts = [Third(c) for c in range(chunks)]
-    early = x_at > 0
+    early = x_at >= row_n // 2
 
     def fold_at(stage, who):
         @pl.when(who)
@@ -461,13 +469,14 @@
             stage()
 
     for c in reversed(range(chunks)):
+        if c == 2:
+            fold_at(fold_row, early)
         if c == 1:
             pool_out(0).start()
-            fold_at(fold_row, early)
+            fold_at(fold_row, jnp.logical_not(early))
         if c == 0:
             pool_out(1).start()
-            fold_at(fold_column, early)
-            fold_at(fold_row, jnp.logical_not(early))
+            fold_at(fold_column, x_at > 0)
 
             @pl.when(sp > 0)
             def _():
@@ -484,7 +493,7 @@
             parts[c].mixed()
             parts[c].score()
     pool_out(2).start()
-    fold_at(fold_column, jnp.logical_not(early))
+    fold_at(fold_column, x_at == 0)
 
     with jax.named_scope("wo"):
         pltpu.make_async_copy(wo_buf.at[OWN], wo_buf.at[OWN], wo_loc).wait()
@@ -505,11 +514,10 @@
         pool_part(chunks - 2)
     with jax.named_scope("pool_recv"):
         pool_out(1).wait_recv()
+        pool_out(2).wait_recv()
     with jax.named_scope("pool"):
         pool_part(1)
-
-    with jax.named_scope("pool_recv"):
-        pool_out(2).wait_recv()
+        pool_part(0)
 
     @pl.when(sp > 0)
     def _():
@@ -544,16 +552,16 @@
 
     with jax.named_scope("fourth"):
         fourth(0)
-        pool_part(0)
         fourth(1)
         rec_out(0).start()
+        rec_out(1).start()
     with jax.named_scope("fourth2"):
         fourth(2)
         rec_part(OWN, 0)
-        rec_out(1).start()
+        rec_out(2).start()
         fourth(3)
         rec_part(OWN, 1)
-        rec_out(2).start()
+        rec_out(3).start()
 
     def fold(x):
         acc = x[:, :LANES]
@@ -573,20 +581,19 @@
         stat_own[rows, :] = jnp.where(first_half, sums, squares)
 
     with jax.named_scope("fifth"):
-        rec_out(0).wait_recv()
-        fifth(0)
-        fifth(1)
         rec_part(OWN, 2)
+        rec_part(OWN, 3)
+        for c in range(3):
+            with jax.named_scope("rec_recv"):
+                rec_out(c).wait_recv()
+        for c in range(3):
+            fifth(c)
         s_out(0).start()
-    with jax.named_scope("fifth2"):
-        rec_out(1).wait_recv()
-        fifth(2)
-        rec_part(OWN, 3)
+    with jax.named_scope("fifth3"):
+        with jax.named_scope("rec_recv"):
+            rec_out(3).wait_recv()
+        fifth(3)
         s_out(1).start()
-    with jax.named_scope("fifth3"):
-        rec_out(2).wait_recv()
-        fifth(3)
-        s_out(2).start()
 
     with jax.named_scope("sent"):
         to_peer(x_buf.at[OWN], x_buf.at[PEER], x_send, x_recv.at[0]).wait_send()
@@ -615,14 +622,17 @@
         part = pl.ds(c * rows, rows)
         return pltpu.make_async_copy(o_buf.at[part], out.at[0, part], o_sem.at[c])
 
-    first_half = lax.broadcasted_iota(jnp.int32, (rows, LANES), 1) < LANES // 2
+    half = rows // 2
+    first_half = lax.broadcasted_iota(jnp.int32, (half, LANES), 1) < LANES // 2
     for c in range(pieces):
-        part = slice(c * rows, (c + 1) * rows)
-        both = stats[part, :]
-        mean = jnp.sum(jnp.where(first_half, both, 0.0), axis=1, keepdims=True) / width
-        square = jnp.sum(jnp.where(first_half, 0.0, both), axis=1, keepdims=True) / width
-        inv = lax.rsqrt(square - mean * mean + EPS_NORM)
-        o_buf[part, :] = ((resid[part, :] - mean) * inv * gain[...] + bias[...]).astype(BF16)
+        for k in range(2):
+            part = slice(c * rows + k * half, c * rows + (k + 1) * half)
+            both = stats[part, :]
+            mean = jnp.sum(jnp.where(first_half, both, 0.0), axis=1, keepdims=True) * (1.0 / width)
+            square = jnp.sum(jnp.where(first_half, 0.0, both), axis=1, keepdims=True) * (1.0 / width)
+            inv = lax.rsqrt(square - mean * mean + EPS_NORM)
+            shift = -mean * inv
+            o_buf[part, :] = ((resid[part, :] * inv + shift) * gain[...] + bias[...]).astype(BF16)
         leave(c).start()
     for c in range(pieces):
         leave(c).wait()
@@ -672,8 +682,8 @@
             pltpu.VMEM((1, chans), F32),
             pltpu.VMEM((heads, length), F32),
             pltpu.VMEM((1, DK), F32),
-            dma((2,)), dma, dma((2,)), dma((5,)), dma, dma, dma, dma, dma((6,)),
-            dma, dma, dma, dma, dma, dma, dma, dma, dma, dma((3,)), dma((5,)), pltpu.SemaphoreType.REGULAR,
+            dma((2,)), dma, dma((2,)), dma((5,)), dma, dma, dma, dma, dma((7,)),
+            dma, dma, dma, dma, dma, dma, dma, dma, dma, dma((2,)), dma((5,)), pltpu.SemaphoreType.REGULAR,
         ]
         row = lambda x: x.reshape(1, -1)
         resid, stats = pl.pallas_call(

time: 30.6 us -> 29.5 us (0.964)
  Pallas kernels: 30.3 us -> 29 us
    pallas_call x1, Pallas kernels: 28.4 us -> 27.3 us  [local(): pl.pallas_call(functools.partial(mixer, n_sp, n_tp, rows_x), out_shape=(p...]
where the time goes in v5:
time: 29.5 us; the launch traced here: 29.2 us
  Pallas kernels  29 us (98%)
    pallas_call x1, Pallas kernels, local(): pl.pallas_call(functools.partial(mixer, n_sp, n_tp, rows_x), out_shape=(p...  27.3 us
    pallas_call x1, Pallas kernels, local(): pl.pallas_call(functools.partial(finish, n_tp * feats, piece), out_shape=...  1.66 us

profile of v5, /device:TPU:81, one launch (start us, length us, event | category | flops | bytes accessed | tf_op | source)
XLA Modules:
  0.0 29.2 jit_solution(15767227177101269327)
XLA Ops:
  0.0 0.0 copy-start
  0.0 0.0 copy-start.1
  0.0 27.3 %mixer.1 = (f32[1024,1024]{1,0:T(8,128)S(1)}, f32[1024,128]{1,0:T(8,128)S(1)}) custom-call(bf16[1,1024,1024]{2,1,0:T(8,128)(2,1)} %stream.1, bf16[2048,512]{1,0:T(8,128)(2,1)} %w_pool.1, bf16[2048,512]{1,0:T(8,128)(2,1)} %w_query.1, bf16[2048,512]{1,0:T(8,128)(2,1)} %w_forget.1, bf16[2048,512]{1,0:T(8,128)(2,1)} %w_value.1, bf16[2048,512]{1,0:T(8,128)(2,1)} %w_gate.1, ...), custom_call_target="tpu_custom_call" | custom-call | tf_op jit(solution)/shard_map/mixer/pallas_call | solution.py:689
  27.3 0.0 copy-done
  27.4 0.0 copy-done.1
  27.4 1.7 %finish.1 = bf16[1,1024,1024]{2,1,0:T(8,128)(2,1)} custom-call(f32[1024,1024]{1,0:T(8,128)S(1)} %get-tuple-element.7.resid, f32[1024,128]{1,0:T(8,128)S(1)} %get-tuple-element.8.stats, f32[1,1024]{1,0:T(1,128)S(1)} %bitcast.6, f32[1,1024]{1,0:T(1,128)S(1)} %bitcast.7), custom_call_target="tpu_custom_call" | custom-call | tf_op jit(solution)/shard_map/finish/pallas_call | solution.py:702
Async XLA Ops:
  0.0 27.3 %copy-start = (f32[1024]{0:T(1024)S(1)}, f32[1024]{0:T(1024)}, u32[]{:S(2)}) copy-start(f32[1024]{0:T(1024)} %param.28) | copy-start | bytes 12292
  0.0 27.4 %copy-start.1 = (f32[1024]{0:T(1024)S(1)}, f32[1024]{0:T(1024)}, u32[]{:S(2)}) copy-start(f32[1024]{0:T(1024)} %param.29) | copy-start | bytes 12292
